TPU v7x, 32 devices: a whole 2x2x4 slice. The times are simulated.
32 devices in a mesh: sp: 4 (over y, x), tp: 8 (over z, core).
Axes of the slice: x: 2, y: 2, z: 4, core: 2. Of those that a mesh axis runs over, the one named last changes fastest.
Arguments:
- conv_outer: bfloat16 [2048, 1024], P('tp', 'sp'), may hold values from -6 to 6
- conv_inner: bfloat16 [2048, 1024], P('tp', 'sp'), may hold values from -6 to 6
- conv_input: bfloat16 [2048, 1024], P('tp', 'sp'), may hold values from -6 to 6
- conv_taps: float32 [3, 2048], P(None, 'tp'), may hold values from -3 to 3
- out_proj: bfloat16 [2048, 4096], P('tp'), may hold values from -0.125 to 0.125
- mixed_state: bfloat16 [1024, 4096], P('sp', 'tp'), may hold values from -6 to 6
- route_ids: int32 [1024, 2], P('sp'), may hold values from 0 to 3, all different within a row; in each aligned block of 256 rows (0 to 255, 256 to 511, ...) at most 256 rows name the same one
- route_weights: float32 [1024, 2], P('sp'), may hold values from 0.1 to 1
- w_gate: bfloat16 [4, 2048, 4096], P('sp', 'tp'), may hold values from -0.09375 to 0.09375
- w_up: bfloat16 [4, 2048, 4096], P('sp', 'tp'), may hold values from -0.09375 to 0.09375
- w_down: bfloat16 [4, 2048, 4096], P('sp', 'tp'), may hold values from -0.125 to 0.125
- cotangent: bfloat16 [1024, 4096], P('sp', 'tp'), may hold values from -8 to 8
Outputs:
- grad_gate: float32 [4, 2048, 4096], P('sp', 'tp')
- grad_up: float32 [4, 2048, 4096], P('sp', 'tp')
- grad_down: float32 [4, 2048, 4096], P('sp', 'tp')
- grad_mixed: bfloat16 [1024, 4096], P('sp', 'tp')
- grad_proj: float32 [2048, 4096], P('tp', 'sp')
- grad_outer: bfloat16 [2048, 1024], P('tp', 'sp')
- grad_inner: bfloat16 [2048, 1024], P('tp', 'sp')
- grad_input: bfloat16 [2048, 1024], P('tp', 'sp')
Inputs may be any that keep to these rules, and one draw needn't show every extreme that they name: `route_ids`: each row names 2 different experts; among the tokens of one index of sp no expert is named more than 256 times, a bound that some block reaches.
All inputs are finite; a program needn't handle non-finite values.
Results may differ from a plain program's by a relative error of at most 0.022.
Values may be sent and summed in bfloat16 or wider, within the bound.
A program may use at most 128 MiB of HBM per device.

v0:
```python
import functools

import jax
import jax.numpy as jnp
from jax import lax
from jax.experimental import pallas as pl
from jax.experimental.pallas import tpu as pltpu
from jax.sharding import PartitionSpec as P


def from_behind(value, axis, steps):
    count = lax.axis_size(axis)
    first, last = (max(0, -steps), min(count, count - steps))
    return lax.ppermute(value, axis, [(source, source + steps) for source in range(first, last)])


def row_back_kernel(gate_ref, up_ref, gate_w_ref, up_w_ref, out_ref):
    total = jnp.dot(gate_ref[...], gate_w_ref[...], preferred_element_type=jnp.float32)
    total += jnp.dot(up_ref[...], up_w_ref[...], preferred_element_type=jnp.float32)
    out_ref[...] = total.astype(out_ref.dtype)


def row_back(back_gate, back_up, gate_w, up_w):
    rows, hidden = back_gate.shape
    width = gate_w.shape[1]
    tile = min(512, width)
    left = pl.BlockSpec((rows, hidden), lambda i: (0, 0))
    right = pl.BlockSpec((hidden, tile), lambda i: (0, i))
    return pl.pallas_call(
        row_back_kernel,
        grid=(width // tile,),
        out_shape=jax.ShapeDtypeStruct((rows, width), jnp.bfloat16),
        in_specs=[left, left, right, right],
        out_specs=pl.BlockSpec((rows, tile), lambda i: (0, i)),
        cost_estimate=pl.CostEstimate(
            flops=4 * rows * hidden * width,
            bytes_accessed=2 * (2 * rows * hidden + 2 * hidden * width + rows * width),
            transcendentals=0,
        ),
        name="row_back",
    )(back_gate, back_up, gate_w, up_w)


def expert_step(rows_in, rows_grad, gate_w, up_w, down_w):
    gate_pre = jnp.einsum("rd,fd->rf", rows_in, gate_w, preferred_element_type=jnp.float32)
    up_pre = jnp.einsum("rd,fd->rf", rows_in, up_w, preferred_element_type=jnp.float32)
    sig_gate = jax.nn.sigmoid(gate_pre)
    silu_gate = gate_pre * sig_gate
    hidden = (silu_gate * up_pre).astype(jnp.bfloat16)
    back_hidden = jnp.einsum("rd,fd->rf", rows_grad, down_w, preferred_element_type=jnp.float32)
    back_gate = (back_hidden * up_pre * sig_gate * (1.0 + gate_pre * (1.0 - sig_gate))).astype(
        jnp.bfloat16
    )
    back_up = (back_hidden * silu_gate).astype(jnp.bfloat16)
    grad_down_e = jnp.einsum("rf,rd->fd", hidden, rows_grad, preferred_element_type=jnp.float32)
    grad_gate_e = jnp.einsum("rf,rd->fd", back_gate, rows_in, preferred_element_type=jnp.float32)
    grad_up_e = jnp.einsum("rf,rd->fd", back_up, rows_in, preferred_element_type=jnp.float32)
    partial_value = row_back(back_gate, back_up, gate_w, up_w)
    return (partial_value, grad_gate_e, grad_up_e, grad_down_e)


Z_UP, Z_DOWN, BY_X, BY_Y, HALF_X, HALF_Y, PEER = range(7)
KINDS = PEER + 4


def gather_kernel(levels, cot_in, state_in, cot_out, state_out, own_sem, send_sem, recv_sem):
    sp, tp = lax.axis_index("sp"), lax.axis_index("tp")
    level, core = tp // 2, tp % 2
    beside_x = sp + 1 - 2 * (sp % 2)
    beside_y = (sp + 2) % 4
    across = 3 - sp
    peer = tp + 1 - 2 * core
    rows, cols = cot_in.shape
    half = rows // 2
    ins, outs = (cot_in, state_in), (cot_out, state_out)

    barrier = pltpu.get_barrier_semaphore()

    def greet(to_sp, to_tp):
        pl.semaphore_signal(
            barrier,
            inc=1,
            device_id=(to_sp, to_tp),
            device_id_type=pl.DeviceIdType.MESH,
        )

    greet(beside_x, tp)
    greet(beside_y, tp)
    greet(sp, peer)
    pl.when(level > 0)(lambda: greet(sp, tp - 2))
    pl.when(level < levels - 1)(lambda: greet(sp, tp + 2))
    one = jnp.int32(1)
    none = jnp.int32(0)
    pl.semaphore_wait(
        barrier,
        3 + jnp.where(level > 0, one, none) + jnp.where(level < levels - 1, one, none),
    )

    def block(array, of_sp, of_level, of_core, start=0, size=rows):
        return outs[array].at[
            pl.ds(pl.multiple_of(of_sp * rows + start, 16), size),
            pl.ds(pl.multiple_of((of_level * 2 + of_core) * cols, 128), cols),
        ]

    def remote(array, kind, of_level, source, target, to_sp, to_tp):
        return pltpu.make_async_remote_copy(
            src_ref=source,
            dst_ref=target,
            send_sem=send_sem.at[array, kind, of_level],
            recv_sem=recv_sem.at[array, kind, of_level],
            device_id=(to_sp, to_tp),
            device_id_type=pl.DeviceIdType.MESH,
        )

    def spread(array, of_level, source, kind, to_sp, to_tp):
        remote(
            array, kind, of_level, source, block(array, sp, of_level, core), to_sp, to_tp
        ).start()

    def pieces(array, of_level):
        return {
            Z_UP: block(array, sp, of_level, core),
            Z_DOWN: block(array, sp, of_level, core),
            BY_X: block(array, beside_x, of_level, core),
            BY_Y: block(array, beside_y, of_level, core),
            HALF_Y: block(array, across, of_level, core, 0, half),
            HALF_X: block(array, across, of_level, core, half, half),
            PEER: block(array, sp, of_level, 1 - core),
            PEER + 1: block(array, beside_x, of_level, 1 - core),
            PEER + 2: block(array, beside_y, of_level, 1 - core),
            PEER + 3: block(array, across, of_level, 1 - core),
        }

    def arrive(array, kind, of_level):
        piece = pieces(array, of_level)[kind]
        remote(array, kind, of_level, piece, piece, sp, peer).wait_recv()

    def left(array, kind, of_level):
        piece = pieces(array, of_level)[kind]
        remote(array, kind, of_level, piece, piece, sp, peer).wait_send()

    def hand_on(array, of_level, kind, of_sp, to_sp, to_tp, start=0, size=rows):
        piece = block(array, of_sp, of_level, core, start, size)
        remote(array, kind, of_level, piece, piece, to_sp, to_tp).start()

    def column(array, step, up):
        of_level = level if step == 0 else (level - step if up else level + step)
        if step == 0:
            source = ins[array]
            pltpu.make_async_copy(
                source, block(array, sp, level, core), own_sem.at[array]
            ).start()
        else:
            arrive(array, Z_UP if up else Z_DOWN, of_level)
            source = block(array, sp, of_level, core)
        if step == 0 or up:
            pl.when(level < levels - 1)(
                lambda: spread(array, of_level, source, Z_UP, sp, tp + 2)
            )
        if step == 0 or not up:
            pl.when(level > 0)(lambda: spread(array, of_level, source, Z_DOWN, sp, tp - 2))
        spread(array, of_level, source, BY_X, beside_x, tp)
        spread(array, of_level, source, BY_Y, beside_y, tp)
        spread(array, of_level, source, PEER, sp, peer)

    def plane(array, step, up):
        of_level = level - step if up else level + step
        arrive(array, BY_X, of_level)
        hand_on(array, of_level, HALF_Y, beside_x, beside_y, tp, 0, half)
        hand_on(array, of_level, PEER + 1, beside_x, sp, peer)
        arrive(array, BY_Y, of_level)
        hand_on(array, of_level, HALF_X, beside_y, beside_x, tp, half, half)
        hand_on(array, of_level, PEER + 2, beside_y, sp, peer)

    def corner(array, step, up):
        of_level = level - step if up else level + step
        arrive(array, HALF_X, of_level)
        arrive(array, HALF_Y, of_level)
        hand_on(array, of_level, PEER + 3, across, sp, peer)

    def each(action, step):
        if not 0 <= step < levels:
            return
        if step == 0:
            for array in range(2):
                action(array, 0, True)
            return

        @pl.when(level >= step)
        def _():
            for array in range(2):
                action(array, step, True)

        @pl.when(level < levels - step)
        def _():
            for array in range(2):
                action(array, step, False)

    for step in range(levels + 2):
        each(column, step)
        each(plane, step - 1)
        each(corner, step - 2)

    for array in range(2):
        pltpu.make_async_copy(
            ins[array], block(array, sp, level, core), own_sem.at[array]
        ).wait()
        for of_level in range(levels):
            for kind in (PEER, PEER + 1, PEER + 2, PEER + 3):
                arrive(array, kind, of_level)
                left(array, kind, of_level)
            for kind in (BY_X, BY_Y, HALF_X, HALF_Y):
                left(array, kind, of_level)
            pl.when((level < levels - 1) & (level >= of_level))(
                lambda: left(array, Z_UP, of_level)
            )
            pl.when((level > 0) & (level <= of_level))(lambda: left(array, Z_DOWN, of_level))


def gather_all(cotangent, mixed_state):
    rows, cols = cotangent.shape
    levels = lax.axis_size("tp") // 2
    whole = jax.ShapeDtypeStruct((4 * rows, 2 * levels * cols), cotangent.dtype)
    return pl.pallas_call(
        functools.partial(gather_kernel, levels),
        out_shape=(whole, whole),
        in_specs=[pl.BlockSpec(memory_space=pltpu.VMEM)] * 2,
        out_specs=[pl.BlockSpec(memory_space=pl.ANY)] * 2,
        scratch_shapes=[
            pltpu.SemaphoreType.DMA((2,)),
            pltpu.SemaphoreType.DMA((2, KINDS, levels)),
            pltpu.SemaphoreType.DMA((2, KINDS, levels)),
        ],
        compiler_params=pltpu.CompilerParams(collective_id=0, has_side_effects=True),
        name="gather_all",
    )(cotangent, mixed_state)


def sum_blocks(tall, sp_size, rows, cols):
    parts = lax.all_to_all(
        tall.reshape(sp_size, 1, rows, cols), "sp", split_axis=0, concat_axis=0, tiled=True
    )
    return jnp.sum(parts.reshape(sp_size, rows, cols).astype(jnp.float32), axis=0)


def shards(
    conv_outer,
    conv_inner,
    conv_input,
    conv_taps,
    out_proj,
    mixed_state,
    route_ids,
    route_weights,
    w_gate,
    w_up,
    w_down,
    cotangent,
):
    tok_count = mixed_state.shape[0]
    col_count = mixed_state.shape[1]
    top_count = route_ids.shape[1]
    sp_size = lax.axis_size("sp")
    local_experts = w_gate.shape[0]
    experts = local_experts * sp_size
    capacity = 4 * tok_count // experts
    if capacity == tok_count and sp_size == 4 and lax.axis_size("tp") % 2 == 0:
        choice = route_ids[:, :, None] == jnp.arange(experts, dtype=jnp.int32)[None, None, :]
        scale_of = jnp.sum(jnp.where(choice, route_weights[:, :, None], 0.0), axis=1).T
        scales = lax.all_to_all(
            scale_of[:, None], "sp", split_axis=0, concat_axis=1, tiled=True
        ).reshape(-1, 1)
        cot_all, rows_in = gather_all(cotangent, mixed_state)
        rows_grad = (cot_all.astype(jnp.float32) * scales).astype(jnp.bfloat16)
        partial_value, grad_gate_e, grad_up_e, grad_down_e = expert_step(
            rows_in, rows_grad, w_gate[0], w_up[0], w_down[0]
        )
        tall = lax.psum_scatter(
            partial_value, "tp", scatter_dimension=1, tiled=True
        )
        tall, grad_gate_e, grad_up_e, grad_down_e = lax.optimization_barrier(
            (tall, grad_gate_e, grad_up_e, grad_down_e)
        )
        summed = sum_blocks(tall, sp_size, tok_count, col_count)
        grad_mixed = (cotangent.astype(jnp.float32) + summed).astype(jnp.bfloat16)
    else:
        flat_ids = route_ids.reshape(-1)
        onehot = (flat_ids[:, None] == jnp.arange(experts, dtype=jnp.int32)[None, :]).astype(jnp.int32)
        slot_pos = jnp.sum(jnp.cumsum(onehot, axis=0) * onehot, axis=1) - 1
        slot_dest = flat_ids * capacity + slot_pos
        token_of = jnp.arange(flat_ids.shape[0], dtype=jnp.int32) // top_count
        scale_flat = route_weights.reshape(-1)[:, None]

        def pack_rows(rows):
            buffer = jnp.zeros((experts * capacity, rows.shape[1]), rows.dtype).at[slot_dest].set(rows)
            return buffer.reshape(sp_size, local_experts, capacity, rows.shape[1])

        sent_state = pack_rows(mixed_state[token_of])
        sent_grad = pack_rows(
            (cotangent[token_of].astype(jnp.float32) * scale_flat).astype(jnp.bfloat16)
        )
        recv_state, recv_grad = (
            lax.all_to_all(sent_state, "sp", split_axis=0, concat_axis=0, tiled=True),
            lax.all_to_all(sent_grad, "sp", split_axis=0, concat_axis=0, tiled=True),
        )
        state_rows, grad_rows = (
            lax.all_gather(recv_state[:, 0], "tp", axis=2, tiled=True),
            lax.all_gather(recv_grad[:, 0], "tp", axis=2, tiled=True),
        )
        width = state_rows.shape[2]
        rows_in = state_rows.reshape(-1, width)
        rows_grad = grad_rows.reshape(-1, width)
        partial_value, grad_gate_e, grad_up_e, grad_down_e = expert_step(
            rows_in, rows_grad, w_gate[0], w_up[0], w_down[0]
        )
        summed = lax.psum_scatter(
            partial_value, "tp", scatter_dimension=1, tiled=True
        )
        back_rows = summed.reshape(sp_size, capacity, col_count)
        arrived = lax.all_to_all(
            back_rows[:, None], "sp", split_axis=0, concat_axis=0, tiled=True
        ).reshape(experts * capacity, col_count)
        picked = arrived[slot_dest].astype(jnp.float32).reshape(tok_count, top_count, col_count)
        grad_mixed = (cotangent.astype(jnp.float32) + jnp.sum(picked, axis=1)).astype(jnp.bfloat16)
    taps_count = conv_taps.shape[0]
    rim_width = taps_count - 1
    head_block = from_behind(
        jnp.stack([conv_inner[:, tok_count - rim_width :], conv_input[:, tok_count - rim_width :]]),
        "sp",
        1,
    )
    inner_ext = jnp.concatenate([head_block[0], conv_inner], axis=1).astype(jnp.float32)
    input_ext = jnp.concatenate([head_block[1], conv_input], axis=1).astype(jnp.float32)
    inner_prod = inner_ext * input_ext
    conv_out = jnp.zeros((conv_inner.shape[0], tok_count), jnp.float32)
    for offset in range(taps_count):
        conv_out = (
            conv_out + conv_taps[offset][:, None] * inner_prod[:, offset : offset + tok_count]
        )
    outer_f = conv_outer.astype(jnp.float32)
    mixer_act = (outer_f * conv_out).astype(jnp.bfloat16)
    full_back = lax.all_gather(grad_mixed, "tp", axis=1, tiled=True)
    back_mixer = jnp.einsum("cd,td->ct", out_proj, full_back, preferred_element_type=jnp.float32)
    proj_term = jnp.dot(mixer_act, full_back, preferred_element_type=jnp.float32)
    grad_proj = lax.psum_scatter(
        proj_term.astype(jnp.bfloat16), "sp", scatter_dimension=1, tiled=True
    ).astype(jnp.float32)
    grad_outer = (back_mixer * conv_out).astype(jnp.bfloat16)
    back_conv = back_mixer * outer_f
    tail_back = from_behind(back_conv[:, :rim_width], "sp", -1)
    back_ext = jnp.concatenate([back_conv, tail_back], axis=1)
    back_prod = jnp.zeros_like(back_conv)
    for offset in range(taps_count):
        shift_by = rim_width - offset
        back_prod = (
            back_prod + conv_taps[offset][:, None] * back_ext[:, shift_by : shift_by + tok_count]
        )
    grad_inner = (back_prod * conv_input.astype(jnp.float32)).astype(jnp.bfloat16)
    grad_input = (back_prod * conv_inner.astype(jnp.float32)).astype(jnp.bfloat16)
    return (
        grad_gate_e[None],
        grad_up_e[None],
        grad_down_e[None],
        grad_mixed,
        grad_proj,
        grad_outer,
        grad_inner,
        grad_input,
    )


def solution(mesh):
    placed = (
        P("tp", "sp"),
        P("tp", "sp"),
        P("tp", "sp"),
        P(None, "tp"),
        P("tp", None),
        P("sp", "tp"),
        P("sp", None),
        P("sp", None),
        P("sp", "tp", None),
        P("sp", "tp", None),
        P("sp", "tp", None),
        P("sp", "tp"),
    )
    return jax.shard_map(
        shards,
        mesh=mesh,
        in_specs=placed,
        out_specs=(
            P("sp", "tp", None),
            P("sp", "tp", None),
            P("sp", "tp", None),
            P("sp", "tp"),
            P("tp", "sp"),
            P("tp", "sp"),
            P("tp", "sp"),
            P("tp", "sp"),
        ),
        check_vma=False,
    )
```

profile of v0, /device:TPU:7, one launch (start us, length us, event | category | flops | bytes accessed | tf_op | source)
XLA Modules:
  0.0 297.8 jit_solution(3956854586350003306)
XLA Ops:
  7.2 0.0 copy-start
  7.2 0.9 select_reduce_fusion
  8.0 0.6 copy.57
  8.6 3.6 %all-to-all-start = ((f32[4,1,256]{2,1,0:T(1,128)}), f32[4,1,256]{2,1,0:T(1,128)S(1)}, u32[]{:S(2)}, u32[]{:S(2)}) async-start(f32[4,1,256]{2,1,0:T(1,128)} %copy.57), calls=%async_computation | async-start | bytes 8192 | tf_op jit(solution)/shard_map/all_to_all | solution.py:270
  12.3 0.0 reduce-scatter.3.cloned.1.call-start
  12.3 74.6 %gather_all.1 = (bf16[1024,4096]{1,0:T(8,128)(2,1)}, bf16[1024,4096]{1,0:T(8,128)(2,1)}) custom-call(bf16[256,512]{1,0:T(8,128)(2,1)} %cot_in.1, bf16[256,512]{1,0:T(8,128)(2,1)} %state_in.1), custom_call_target="tpu_custom_call" | custom-call | tf_op jit(solution)/shard_map/gather_all/pallas_call | solution.py:224
  86.9 0.0 copy-start.10
  86.9 6.5 %fusion.14 = f32[1024,256]{1,0:T(8,128)S(1)} fusion(bf16[1024,4096]{1,0:T(8,128)(2,1)} %get-tuple-element.15, bf16[1,256,4096]{2,1,0:T(8,128)(2,1)} %param.20), kind=kOutput, calls=%fused_computation.40 | convolution fusion | flops 2147483648 | bytes 11534336 | tf_op jit(solution)/shard_map/rd,fd->rf/dot_general | solution.py:45
  93.4 0.4 copy-done.10
  93.8 3.3 %fusion.16 = f32[1024,256]{1,0:T(8,128)} fusion(bf16[1024,4096]{1,0:T(8,128)(2,1)S(1)} %copy-done.1, bf16[1,256,4096]{2,1,0:T(8,128)(2,1)S(1)} %copy-done.10), kind=kOutput, calls=%fused_computation.42 | convolution fusion | flops 2147483648 | bytes 11534336 | tf_op jit(solution)/shard_map/rd,fd->rf/dot_general | solution.py:46
  97.2 0.0 all-to-all-done
  97.2 0.0 copy-done.11
  97.2 7.2 %multiply_convert_fusion.4 = (bf16[1024,256]{1,0:T(8,128)(2,1)}, bf16[1024,256]{1,0:T(8,128)(2,1)}) fusion(f32[1024,256]{1,0:T(8,128)S(1)} %fusion.14, f32[1024,256]{1,0:T(8,128)} %fusion.16, bf16[1,256,4096]{2,1,0:T(8,128)(2,1)S(1)} %copy-done, bf16[1024,4096]{1,0:T(8,128)(2,1)} %get-tuple-element.14, f32[1024]{0:T(1024)S(1)} %bitcast.53), kind=kOutput, calls=%fused_computation.8 | convolution fusion | flops 2163474432 | bytes 13635584 | tf_op jit(solution)/shard_map/rd,fd->rf/dot_general | solution.py:50
  104.4 10.3 %row_back.1 = bf16[1024,4096]{1,0:T(8,128)(2,1)} custom-call(bf16[1024,256]{1,0:T(8,128)(2,1)} %get-tuple-element.57.gate_ref, bf16[1024,256]{1,0:T(8,128)(2,1)} %get-tuple-element.56.up_ref, bf16[256,4096]{1,0:T(8,128)(2,1)} %bitcast.57, bf16[256,4096]{1,0:T(8,128)(2,1)} %bitcast.58), custom_call_target="tpu_custom_call" | custom-call | flops 4294967296 | bytes 13631488 | tf_op jit(solution)/shard_map/row_back/pallas_call | solution.py:29
  114.8 0.0 reduce-scatter.3.cloned.1.call-update
  114.8 0.0 copy-start.4
  114.8 0.2 all-gather.2.cloned.1.call-start
  115.0 0.8 copy-done.5
  115.8 7.9 %fusion.23 = f32[256,4096]{1,0:T(8,128)} fusion(bf16[1024,256]{1,0:T(8,128)(2,1)S(1)} %copy-done.5, bf16[1024,4096]{1,0:T(8,128)(2,1)} %get-tuple-element.15), kind=kOutput, calls=%fused_computation.47 | convolution fusion | flops 2147483648 | bytes 13107200 | tf_op jit(solution)/shard_map/rf,rd->fd/dot_general | solution.py:57
  123.8 7.9 %fusion.22 = f32[256,4096]{1,0:T(8,128)} fusion(bf16[1024,256]{1,0:T(8,128)(2,1)S(1)} %copy-done.4, bf16[1024,4096]{1,0:T(8,128)(2,1)} %get-tuple-element.15), kind=kOutput, calls=%fused_computation.46 | convolution fusion | flops 2147483648 | bytes 13107200 | tf_op jit(solution)/shard_map/rf,rd->fd/dot_general | solution.py:56
  131.7 0.0 slice-done
  131.7 0.0 copy-start.3
  131.7 5.0 %fusion = f32[256,4096]{1,0:T(8,128)} fusion(bf16[1024,4096]{1,0:T(8,128)(2,1)S(1)} %bitcast.56, f32[1024]{0:T(1024)S(1)} %bitcast.54, f32[1024,256]{1,0:T(8,128)S(1)} %copy-done.13, f32[1024,256]{1,0:T(8,128)S(1)} %copy-done.12), kind=kOutput, calls=%fused_computation.2 | convolution fusion | flops 2161639424 | bytes 14684160 | tf_op jit(solution)/shard_map/rf,rd->fd/dot_general | solution.py:55
  136.7 66.5 %reduce-scatter.3.cloned.1.call-done = bf16[1024,512]{1,0:T(8,128)(2,1)} async-done(((bf16[1024,4096]{1,0:T(8,128)(2,1)}), bf16[1024,512]{1,0:T(8,128)(2,1)}) %reduce-scatter.3.cloned.1.call-update) | async-done | bytes 1048592 | tf_op jit(solution)/shard_map/reduce_scatter | solution.py:278
  203.2 13.6 %all_to_all.14 = bf16[4,1,256,512]{3,2,1,0:T(8,128)(2,1)S(1)} all-to-all(bf16[4,1,256,512]{3,2,1,0:T(8,128)(2,1)} %bitcast.45), channel_id=1, replica_groups=mesh['sp'=4,'tp'=8] {'sp'}, dimensions={0} | all-to-all | bytes 2097152 | tf_op jit(solution)/shard_map/all_to_all | solution.py:240
  216.8 0.1 convert_reduce_fusion
  217.0 0.0 copy-done.3
  217.0 0.8 add_convert_fusion
  217.8 0.0 all-gather.2.cloned.1.call-update
  217.8 0.0 reduce-scatter.5.cloned.1.call-start
  217.8 0.1 copy.60
  218.0 0.1 copy.61
  218.1 1.3 collective-permute-start
  219.4 0.1 copy.59
  219.5 2.9 collective-permute-done
  222.4 0.1 convert_multiply_fusion.2
  222.5 28.2 %all-gather.2.cloned.1.call-done = bf16[256,4096]{1,0:T(8,128)(2,1)} async-done(((bf16[256,512]{1,0:T(8,128)(2,1)}), bf16[256,4096]{1,0:T(8,128)(2,1)}) %all-gather.2.cloned.1.call-update) | async-done | bytes 2097168 | tf_op jit(solution)/shard_map/all_gather | solution.py:342
  250.7 3.1 %multiply_convert_fusion.9 = (bf16[256,256]{0,1:T(8,128)(2,1)S(1)}, f32[256,256]{0,1:T(8,128)S(1)}, f32[256,256]{0,1:T(8,128)S(1)}) fusion(f32[256,258]{0,1:T(8,128)S(1)} %convert_multiply_fusion.2, f32[256]{0:T(256)S(1)} %bitcast.49, f32[256]{0:T(256)S(1)} %bitcast.51, f32[256]{0:T(256)S(1)} %bitcast.47, bf16[256,256]{0,1:T(8,128)(2,1)S(1)} %copy.59, ...), kind=kOutput, calls=%fused_computation.32 | convolution fusion | flops 537460736 | bytes 5770240 | tf_op jit(solution)/shard_map/cd,td->ct/dot_general | solution.py:343
  253.8 2.1 convolution_convert_fusion
  255.9 0.0 reduce-scatter.5.cloned.1.call-update
  255.9 2.2 collective-permute-start.1
  258.1 0.8 copy.66
  258.9 0.0 collective-permute-done.1
  258.9 0.1 multiply_convert_fusion.7
  259.0 0.8 copy.68
  259.8 0.8 copy.67
  260.6 28.6 %reduce-scatter.5.cloned.1.call-done = bf16[256,1024]{1,0:T(8,128)(2,1)} async-done(((bf16[256,4096]{1,0:T(8,128)(2,1)}), bf16[256,1024]{1,0:T(8,128)(2,1)}) %reduce-scatter.5.cloned.1.call-update) | async-done | bytes 524304 | tf_op jit(solution)/shard_map/reduce_scatter | solution.py:345
  289.2 2.1 convert_element_type.71
  (30 shorter events, 0.1 us)
Async XLA Ops:
  7.2 90.0 %copy-start = (bf16[1,256,4096]{2,1,0:T(8,128)(2,1)S(1)}, bf16[1,256,4096]{2,1,0:T(8,128)(2,1)}, u32[]{:S(2)}) copy-start(bf16[1,256,4096]{2,1,0:T(8,128)(2,1)} %param.22) | copy-start | bytes 6291460
  8.6 88.5 %all-to-all-start = ((f32[4,1,256]{2,1,0:T(1,128)}), f32[4,1,256]{2,1,0:T(1,128)S(1)}, u32[]{:S(2)}, u32[]{:S(2)}) async-start(f32[4,1,256]{2,1,0:T(1,128)} %copy.57), calls=%async_computation | async-start | bytes 8192 | tf_op jit(solution)/shard_map/all_to_all | solution.py:270
  12.3 191.0 %reduce-scatter.3.cloned.1.call-start = ((), (), s32[]{:S(2)}) async-start(), calls=%async_computation.4 | async-start | bytes 9437184 | tf_op jit(solution)/shard_map/reduce_scatter | solution.py:278
  86.9 6.5 %copy-start.1 = (bf16[1024,4096]{1,0:T(8,128)(2,1)S(1)}, bf16[1024,4096]{1,0:T(8,128)(2,1)}, u32[]{:S(2)}) copy-start(bf16[1024,4096]{1,0:T(8,128)(2,1)} %get-tuple-element.15) | copy-start | bytes 25165828
  86.9 7.0 %copy-start.10 = (bf16[1,256,4096]{2,1,0:T(8,128)(2,1)S(1)}, bf16[1,256,4096]{2,1,0:T(8,128)(2,1)}, u32[]{:S(2)}) copy-start(bf16[1,256,4096]{2,1,0:T(8,128)(2,1)} %param.21) | copy-start | bytes 6291460
  93.8 3.4 %copy-start.11 = (f32[1024,256]{1,0:T(8,128)}, f32[1024,256]{1,0:T(8,128)S(1)}, u32[]{:S(2)}) copy-start(f32[1024,256]{1,0:T(8,128)S(1)} %fusion.14) | copy-start | bytes 3145732
  114.8 1.0 copy-start.5
  114.8 8.9 %copy-start.4 = (bf16[1024,256]{1,0:T(8,128)(2,1)S(1)}, bf16[1024,256]{1,0:T(8,128)(2,1)}, u32[]{:S(2)}) copy-start(bf16[1024,256]{1,0:T(8,128)(2,1)} %get-tuple-element.57.gate_ref) | copy-start | bytes 1572868
  114.8 135.9 %all-gather.2.cloned.1.call-start = ((), (), s32[]{:S(2)}) async-start(), calls=%async_computation.5 | async-start | bytes 2359296 | tf_op jit(solution)/shard_map/all_gather | solution.py:342
  115.8 15.9 %slice-start = ((s8[8388608]{0:T(1024)(128)(4,1)}), s8[4194304]{0:T(1024)(128)(4,1)S(1)}, s32[]{:S(2)}) async-start(s8[8388608]{0:T(1024)(128)(4,1)} %bitcast.55), calls=%async_computation.7 | async-start | bytes 8388608
  123.7 8.0 %slice-start.1 = ((s8[8388608]{0:T(1024)(128)(4,1)}), s8[4194304]{0:T(1024)(128)(4,1)S(1)}, s32[]{:S(2)}) async-start(s8[8388608]{0:T(1024)(128)(4,1)} %bitcast.55), calls=%async_computation.8 | async-start | bytes 8388608
  123.7 8.0 %copy-start.12 = (f32[1024,256]{1,0:T(8,128)S(1)}, f32[1024,256]{1,0:T(8,128)}, u32[]{:S(2)}) copy-start(f32[1024,256]{1,0:T(8,128)} %copy-done.11) | copy-start | bytes 3145732
  123.7 8.0 %copy-start.13 = (f32[1024,256]{1,0:T(8,128)S(1)}, f32[1024,256]{1,0:T(8,128)}, u32[]{:S(2)}) copy-start(f32[1024,256]{1,0:T(8,128)} %fusion.16) | copy-start | bytes 3145732
  131.7 85.3 %copy-start.3 = (bf16[256,512]{1,0:T(8,128)(2,1)S(1)}, bf16[256,512]{1,0:T(8,128)(2,1)}, u32[]{:S(2)}) copy-start(bf16[256,512]{1,0:T(8,128)(2,1)} %cot_in.1) | copy-start | bytes 786436
  136.7 81.1 %copy-start.6 = (bf16[256,256]{1,0:T(8,128)(2,1)S(1)}, bf16[256,256]{1,0:T(8,128)(2,1)}, u32[]{:S(2)}) copy-start(bf16[256,256]{1,0:T(8,128)(2,1)} %param.13) | copy-start | bytes 393220
  136.7 81.2 %copy-start.7 = (bf16[256,256]{1,0:T(8,128)(2,1)S(1)}, bf16[256,256]{1,0:T(8,128)(2,1)}, u32[]{:S(2)}) copy-start(bf16[256,256]{1,0:T(8,128)(2,1)} %param.14) | copy-start | bytes 393220
  136.7 82.7 %copy-start.9 = (f32[3,256]{1,0:T(4,128)S(1)}, f32[3,256]{1,0:T(4,128)}, u32[]{:S(2)}) copy-start(f32[3,256]{1,0:T(4,128)} %param.15) | copy-start | bytes 9220
  136.7 82.7 %copy-start.8 = (bf16[256,256]{1,0:T(8,128)(2,1)S(1)}, bf16[256,256]{1,0:T(8,128)(2,1)}, u32[]{:S(2)}) copy-start(bf16[256,256]{1,0:T(8,128)(2,1)} %param.12) | copy-start | bytes 393220
  217.8 71.4 %reduce-scatter.5.cloned.1.call-start = ((), (), s32[]{:S(2)}) async-start(), calls=%async_computation.6 | async-start | bytes 2621440 | tf_op jit(solution)/shard_map/reduce_scatter | solution.py:345
  218.1 4.3 %collective-permute-start = (bf16[2,256,2]{1,2,0:T(2,128)(2,1)S(1)}, bf16[2,256,2]{1,2,0:T(2,128)(2,1)S(1)}, u32[]{:S(2)}, u32[]{:S(2)}) collective-permute-start(bf16[2,256,2]{1,2,0:T(2,128)(2,1)S(1)} %pad_maximum_fusion.1), channel_id=1, source_target_pairs={{0,8},{8,16},{16,24},{1,9},{9,17},{17,25},{2,10},{10,18},{18,26},{... | collective-permute-start | bytes 6152 | tf_op jit(solution)/shard_map/ppermute | solution.py:14
  250.7 3.1 %copy-start.2 = (bf16[256,4096]{1,0:T(8,128)(2,1)S(1)}, bf16[256,4096]{1,0:T(8,128)(2,1)}, u32[]{:S(2)}) copy-start(bf16[256,4096]{1,0:T(8,128)(2,1)} %all-gather.2.cloned.1.call-done) | copy-start | bytes 6291460
  255.9 3.0 collective-permute-start.1
Sparse Core Ops, SparseCore 0:
  114.9 88.2 reduce-scatter.2
  217.9 32.7 all-gather.1
  256.0 33.0 reduce-scatter.4
where the time goes:
time: 301 us; the launch traced here: 298 us
  waiting for transfers between devices  126 us (42%)
  Pallas kernels  84.9 us (28%)
  matrix products  43.1 us (14%)
  between operations  14 us (5%)
  blocking collectives  13.6 us (5%)
  starting transfers between devices  7.37 us (2%)
  local copies, waits for them, and re-layouts  4.47 us (1%)
  other arithmetic  4.13 us (1%)
    pallas_call x1, Pallas kernels, gather_all(): pl.pallas_call(functools.partial(gather_kernel, levels), out_shape=(whole...  74.6 us
    reduce_scatter x1, waiting for transfers between devices, shards(): lax.psum_scatter(partial_value, 'tp', scatter_dimension=1, tiled=True)  66.5 us
    reduce_scatter x1, waiting for transfers between devices, shards(): lax.psum_scatter(proj_term.astype(jnp.bfloat16), 'sp', scatter_dimension=...  28.6 us
    all_gather x1, waiting for transfers between devices, shards(): full_back = lax.all_gather(grad_mixed, 'tp', axis=1, tiled=True)  28.2 us
    all_to_all x1, blocking collectives, sum_blocks(): lax.all_to_all(tall.reshape(sp_size, 1, rows, cols), 'sp', split_axis=0,...  13.6 us
    pallas_call x1, Pallas kernels, row_back(): pl.pallas_call(row_back_kernel, grid=(width // tile,), out_shape=jax.Shap...  10.3 us
    dot_general x1, matrix products, expert_step(): jnp.einsum('rf,rd->fd', back_gate, rows_in, preferred_element_type=jnp.fl...  7.93 us
    dot_general x1, matrix products, expert_step(): jnp.einsum('rf,rd->fd', back_up, rows_in, preferred_element_type=jnp.floa...  7.93 us
  transfers between devices with their start and end apart: 6, of which 4 were waited for; matrix products, arithmetic and copies ran while one was open for 11% of the time, Pallas kernels for 25%

commit v1 on v0

--- a/solution.py
+++ b/solution.py
@@ -236,14 +236,568 @@
     )(cotangent, mixed_state)
 
 
-def sum_blocks(tall, sp_size, rows, cols):
-    parts = lax.all_to_all(
-        tall.reshape(sp_size, 1, rows, cols), "sp", split_axis=0, concat_axis=0, tiled=True
-    )
-    return jnp.sum(parts.reshape(sp_size, rows, cols).astype(jnp.float32), axis=0)
-
-
-def shards(
+PIECES = 2
+TO_X, TO_Y, PASS_X, PASS_Y, LAST_X, LAST_Y = range(6)
+
+
+def level_at(level, place):
+    inner = (0, 3, 1, 2)[place]
+    high = jnp.where((level == 0) | (level == 3), place, inner)
+    return jnp.where(level >= 2, high, 3 - high)
+
+
+def reduce_kernel(
+    back_in,
+    gate_in,
+    up_in,
+    cot_in,
+    act_in,
+    own_out,
+    token_out,
+    quarter_out,
+    act_out,
+    back,
+    weights,
+    part,
+    passed,
+    landed,
+    plane_sum,
+    z_send,
+    z_land,
+    own_sem,
+    swap_send,
+    swap_recv,
+    plane_send,
+    plane_recv,
+    chain_send,
+    chain_recv,
+    up_send,
+    down_send,
+    spread_recv,
+    peer_send,
+    peer_recv,
+    quarter_send,
+    quarter_recv,
+    mate_send,
+    mate_recv,
+    act_send,
+    act_recv,
+):
+    sp, tp = lax.axis_index("sp"), lax.axis_index("tp")
+    level, core = tp // 2, tp % 2
+    beside_x = sp + 1 - 2 * (sp % 2)
+    beside_y = (sp + 2) % 4
+    across = 3 - sp
+    peer = tp + 1 - 2 * core
+    levels = 4
+    rows, half_cols = cot_in.shape
+    cols = half_cols // PIECES
+    half = rows // 2
+    hidden = gate_in.shape[0]
+    steps = PIECES * levels
+    at_end = (level == 0) | (level == levels - 1)
+
+    barrier = pltpu.get_barrier_semaphore()
+
+    def greet(to_sp, to_tp):
+        pl.semaphore_signal(
+            barrier,
+            inc=1,
+            device_id=(to_sp, to_tp),
+            device_id_type=pl.DeviceIdType.MESH,
+        )
+
+    greet(beside_x, tp)
+    greet(beside_y, tp)
+    greet(across, tp)
+    greet(sp, peer)
+    pl.when(level > 0)(lambda: greet(sp, tp - 2))
+    pl.when(level < levels - 1)(lambda: greet(sp, tp + 2))
+    pl.semaphore_wait(barrier, 6 - jnp.where(at_end, jnp.int32(1), jnp.int32(0)))
+
+    sent = []
+
+    def always(action):
+        action()
+
+    def remote(source, target, send, recv, to_sp, to_tp):
+        return pltpu.make_async_remote_copy(
+            src_ref=source,
+            dst_ref=target,
+            send_sem=send,
+            recv_sem=recv,
+            device_id=(to_sp, to_tp),
+            device_id_type=pl.DeviceIdType.MESH,
+        )
+
+    def send(source, target, send_sem, recv_sem, to_sp, to_tp, when=always):
+        def build():
+            return remote(source, target, send_sem, recv_sem, to_sp, to_tp)
+
+        when(lambda: build().start())
+        sent.append((when, lambda: build().wait_send()))
+
+    def arrive(piece, recv_sem):
+        remote(piece, piece, act_send.at[0], recv_sem, sp, peer).wait_recv()
+
+    mine = pl.ds(0, 2 * hidden)
+    send(back_in, back.at[:, pl.ds(2 * hidden, 2 * hidden)], swap_send.at[0], swap_recv.at[0], sp, peer)
+    pltpu.make_async_copy(back_in, back.at[:, mine], own_sem.at[0]).start()
+
+    def own_weights(place, which):
+        of_level = level_at(level, place)
+        source = (gate_in, up_in)[which].at[
+            :, pl.ds(pl.multiple_of((of_level * 2 + core) * half_cols, 128), half_cols)
+        ]
+        target = weights.at[place, pl.ds(which * hidden, hidden)]
+        return pltpu.make_async_copy(source, target, own_sem.at[1 + 2 * place + which])
+
+    for place in range(levels):
+        for which in range(2):
+            of_level = level_at(level, place)
+            send(
+                (gate_in, up_in)[which].at[
+                    :, pl.ds(pl.multiple_of((of_level * 2 + 1 - core) * half_cols, 128), half_cols)
+                ],
+                weights.at[place, pl.ds((2 + which) * hidden, hidden)],
+                swap_send.at[1 + 2 * place + which],
+                swap_recv.at[1 + 2 * place + which],
+                sp,
+                peer,
+            )
+            own_weights(place, which).start()
+
+    def block(step, of_sp, start, size):
+        return part.at[step, pl.ds(pl.multiple_of(of_sp * rows + start, 128), size)]
+
+    def plane(step, kind, source, to_sp):
+        send(
+            source,
+            landed.at[step, kind],
+            plane_send.at[step, kind],
+            plane_recv.at[step, kind],
+            to_sp,
+            tp,
+        )
+
+    def form(step):
+        piece, place = step // levels, step % levels
+        if step < levels:
+            for which in range(2):
+                own_weights(place, which).wait()
+                arrive(
+                    weights.at[place, pl.ds((2 + which) * hidden, hidden)],
+                    swap_recv.at[1 + 2 * place + which],
+                )
+        if step == 0:
+            pltpu.make_async_copy(back_in, back.at[:, mine], own_sem.at[0]).wait()
+            arrive(back.at[:, pl.ds(2 * hidden, 2 * hidden)], swap_recv.at[0])
+
+        def one(at, _):
+            span = pl.ds(pl.multiple_of(at * rows, 128), rows)
+            part[step, span, :] = jnp.dot(
+                back[span, :],
+                weights[place, :, piece * cols : (piece + 1) * cols],
+                preferred_element_type=jnp.float32,
+            ).astype(part.dtype)
+            return 0
+
+        lax.fori_loop(0, 4, one, 0)
+        plane(step, PASS_X, block(step, across, 0, half), beside_x)
+        plane(step, PASS_Y, block(step, across, half, half), beside_y)
+        plane(step, TO_X, block(step, beside_x, 0, half), beside_x)
+        plane(step, TO_Y, block(step, beside_y, half, half), beside_y)
+
+    def wide(value):
+        return value.astype(jnp.float32)
+
+    def hand_on(step):
+        arrive(landed.at[step, PASS_X], plane_recv.at[step, PASS_X])
+        passed[step, 0] = (
+            wide(block(step, beside_y, 0, half)[...]) + wide(landed[step, PASS_X])
+        ).astype(passed.dtype)
+        plane(step, LAST_Y, passed.at[step, 0], beside_y)
+        arrive(landed.at[step, PASS_Y], plane_recv.at[step, PASS_Y])
+        passed[step, 1] = (
+            wide(block(step, beside_x, half, half)[...]) + wide(landed[step, PASS_Y])
+        ).astype(passed.dtype)
+        plane(step, LAST_X, passed.at[step, 1], beside_x)
+
+    def chain(step, when):
+        piece, place = step // levels, step % levels
+        of_level = level_at(level, place)
+        upward = jnp.where(of_level > level, jnp.int32(1), jnp.int32(0))
+        send(
+            z_send.at[step],
+            z_land.at[piece, of_level, 1 - upward],
+            chain_send.at[step],
+            chain_recv.at[piece, of_level, 1 - upward],
+            sp,
+            tp - 2 + 4 * upward,
+            when,
+        )
+
+    def gather_plane(step):
+        place = step % levels
+        for kind in (TO_X, TO_Y, LAST_X, LAST_Y):
+            arrive(landed.at[step, kind], plane_recv.at[step, kind])
+        low = (
+            wide(block(step, sp, 0, half)[...])
+            + wide(landed[step, TO_X])
+            + wide(landed[step, LAST_Y])
+        )
+        high = (
+            wide(block(step, sp, half, half)[...])
+            + wide(landed[step, TO_Y])
+            + wide(landed[step, LAST_X])
+        )
+        plane_sum[step, :half] = low
+        plane_sum[step, half:] = high
+        if place < levels - 1:
+
+            @pl.when(at_end)
+            def _():
+                z_send[step, :half] = low.astype(z_send.dtype)
+                z_send[step, half:] = high.astype(z_send.dtype)
+
+            chain(step, pl.when(at_end))
+
+    def chained(piece, of_level, way):
+        arrive(z_land.at[piece, of_level, way], chain_recv.at[piece, of_level, way])
+        return wide(z_land[piece, of_level, way])
+
+    def columns(of_level, of_core, piece):
+        return pl.ds(
+            pl.multiple_of((of_level * 2 + of_core) * half_cols + piece * cols, 128), cols
+        )
+
+    def spread_up(piece, of_level, when):
+        view = token_out.at[:, columns(of_level, core, piece)]
+        send(view, view, up_send.at[piece, of_level], spread_recv.at[piece, of_level], sp, tp + 2, when)
+
+    def spread_down(piece, of_level, when):
+        view = token_out.at[:, columns(of_level, core, piece)]
+        send(view, view, down_send.at[piece, of_level], spread_recv.at[piece, of_level], sp, tp - 2, when)
+
+    def quarter(of_sp, of_core, piece):
+        return quarter_out.at[
+            pl.ds(pl.multiple_of(of_sp * rows, 128), rows),
+            pl.ds(pl.multiple_of(of_core * half_cols + piece * cols, 128), cols),
+        ]
+
+    def share(piece, of_level, valid):
+        view = token_out.at[:, columns(of_level, core, piece)]
+        send(
+            view,
+            quarter(sp, core, piece),
+            quarter_send.at[piece, of_level],
+            quarter_recv.at[piece, sp],
+            of_level,
+            tp,
+            pl.when(valid & (of_level != sp)),
+        )
+        send(
+            view,
+            view,
+            peer_send.at[piece, of_level],
+            peer_recv.at[piece, of_level],
+            sp,
+            peer,
+            pl.when(valid),
+        )
+
+    def settle(step):
+        piece, place = step // levels, step % levels
+        if place < levels - 1:
+            of_level = level_at(level, place)
+            upward = jnp.where(of_level > level, jnp.int32(1), jnp.int32(0))
+
+            @pl.when(jnp.logical_not(at_end))
+            def _():
+                total = plane_sum[step] + chained(piece, of_level, 1 - upward)
+                z_send[step] = total.astype(z_send.dtype)
+
+            chain(step, pl.when(jnp.logical_not(at_end)))
+            return
+        span = slice(piece * cols, (piece + 1) * cols)
+        plane_sum[step] += wide(cot_in[:, span])
+
+        @pl.when(level > 0)
+        def _():
+            plane_sum[step] += chained(piece, level, 0)
+
+        @pl.when(level < levels - 1)
+        def _():
+            plane_sum[step] += chained(piece, level, 1)
+
+        result = plane_sum[step].astype(own_out.dtype)
+        own_out[:, span] = result
+        token_out[:, columns(level, core, piece)] = result
+        spread_up(piece, level, pl.when(level < levels - 1))
+        spread_down(piece, level, pl.when(level > 0))
+        share(piece, level, level >= 0)
+
+    def spread(piece, hop):
+        for up in (True, False):
+            of_level = level - hop if up else level + hop
+            valid = of_level >= 0 if up else of_level < levels
+            safe = jnp.where(valid, of_level, level)
+
+            @pl.when(valid)
+            def _():
+                arrive(
+                    token_out.at[:, columns(safe, core, piece)], spread_recv.at[piece, safe]
+                )
+
+            if up:
+                spread_up(piece, safe, pl.when(valid & (level < levels - 1)))
+            else:
+                spread_down(piece, safe, pl.when(valid & (level > 0)))
+            share(piece, safe, valid)
+
+    def mate(piece):
+        for of_sp in (beside_x, beside_y, across):
+            view = quarter(of_sp, core, piece)
+            arrive(view, quarter_recv.at[piece, of_sp])
+            send(view, view, mate_send.at[piece, of_sp], mate_recv.at[piece, of_sp], sp, peer)
+
+    def give_act():
+        for at, to_sp in enumerate((beside_x, beside_y, across)):
+            send(
+                act_in,
+                act_out.at[:, pl.ds(pl.multiple_of(sp * rows, 128), rows)],
+                act_send.at[at],
+                act_recv.at[sp],
+                to_sp,
+                tp,
+            )
+
+    form(0)
+    for turn in range(1, steps + 6):
+        if turn < steps:
+            form(turn)
+        if 0 <= turn - 1 < steps:
+            hand_on(turn - 1)
+        if turn - 1 == steps - 1:
+            give_act()
+        if 0 <= turn - 2 < steps:
+            gather_plane(turn - 2)
+        if 0 <= turn - 3 < steps:
+            settle(turn - 3)
+        for piece in range(PIECES):
+            hop = turn - (piece * levels + levels - 1 + 3)
+            if 1 <= hop < levels:
+                spread(piece, hop)
+    for piece in range(PIECES):
+        mate(piece)
+
+    act_out[:, pl.ds(pl.multiple_of(sp * rows, 128), rows)] = act_in[...]
+    for piece in range(PIECES):
+        for of_level in range(levels):
+            view = token_out.at[:, columns(of_level, 1 - core, piece)]
+            arrive(view, peer_recv.at[piece, of_level])
+        for of_sp in (beside_x, beside_y, across):
+            arrive(quarter(of_sp, 1 - core, piece), mate_recv.at[piece, of_sp])
+    for of_sp in (beside_x, beside_y, across):
+        arrive(
+            act_out.at[:, pl.ds(pl.multiple_of(of_sp * rows, 128), rows)], act_recv.at[of_sp]
+        )
+    quarter_out[pl.ds(pl.multiple_of(sp * rows, 128), rows), :] = token_out[
+        :, pl.ds(pl.multiple_of(sp * 2 * half_cols, 128), 2 * half_cols)
+    ]
+    for when, finish in sent:
+        when(finish)
+
+
+def reduce_all(back, gate_w, up_w, cotangent, act):
+    rows, half_cols = cotangent.shape
+    hidden, width = gate_w.shape
+    steps, cols, half = PIECES * 4, half_cols // PIECES, rows // 2
+    dma = pltpu.SemaphoreType.DMA
+    vmem = pl.BlockSpec(memory_space=pltpu.VMEM)
+    hbm = pl.BlockSpec(memory_space=pl.ANY)
+    narrow = jnp.bfloat16
+    return pl.pallas_call(
+        reduce_kernel,
+        out_shape=(
+            jax.ShapeDtypeStruct((rows, half_cols), narrow),
+            jax.ShapeDtypeStruct((rows, width), narrow),
+            jax.ShapeDtypeStruct((4 * rows, 2 * half_cols), narrow),
+            jax.ShapeDtypeStruct((act.shape[0], 4 * rows), narrow),
+        ),
+        in_specs=[vmem, hbm, hbm, vmem, vmem],
+        out_specs=[vmem] * 4,
+        scratch_shapes=[
+            pltpu.VMEM((4 * rows, 4 * hidden), narrow),
+            pltpu.VMEM((4, 4 * hidden, half_cols), narrow),
+            pltpu.VMEM((steps, 4 * rows, cols), narrow),
+            pltpu.VMEM((steps, 2, half, cols), narrow),
+            pltpu.VMEM((steps, 6, half, cols), narrow),
+            pltpu.VMEM((steps, rows, cols), jnp.float32),
+            pltpu.VMEM((steps, rows, cols), narrow),
+            pltpu.VMEM((PIECES, 4, 2, rows, cols), narrow),
+            dma((9,)),
+            dma((9,)),
+            dma((9,)),
+            dma((steps, 6)),
+            dma((steps, 6)),
+            dma((steps,)),
+            dma((PIECES, 4, 2)),
+            dma((PIECES, 4)),
+            dma((PIECES, 4)),
+            dma((PIECES, 4)),
+            dma((PIECES, 4)),
+            dma((PIECES, 4)),
+            dma((PIECES, 4)),
+            dma((PIECES, 4)),
+            dma((PIECES, 4)),
+            dma((PIECES, 4)),
+            dma((3,)),
+            dma((4,)),
+        ],
+        compiler_params=pltpu.CompilerParams(
+            collective_id=1, has_side_effects=True, vmem_limit_bytes=48 * 1024 * 1024
+        ),
+        name="reduce_all",
+    )(back, gate_w, up_w, cotangent, act)
+
+
+def outer_kernel(hidden_ref, gate_ref, up_ref, state_ref, cot_ref, g_out, u_out, d_out, turned):
+    @pl.when(pl.program_id(0) == 0)
+    def _():
+        turned[0] = hidden_ref[...].T
+        turned[1] = gate_ref[...].T
+        turned[2] = up_ref[...].T
+
+    d_out[...] = jnp.dot(turned[0], cot_ref[...], preferred_element_type=jnp.float32)
+    g_out[...] = jnp.dot(turned[1], state_ref[...], preferred_element_type=jnp.float32)
+    u_out[...] = jnp.dot(turned[2], state_ref[...], preferred_element_type=jnp.float32)
+
+
+def weight_grads(hidden, back_gate, back_up, state, cot):
+    rows, units = hidden.shape
+    width = state.shape[1]
+    tile = min(512, width)
+    whole = pl.BlockSpec((rows, units), lambda i: (0, 0))
+    tall = pl.BlockSpec((rows, tile), lambda i: (0, i))
+    flat = pl.BlockSpec((units, tile), lambda i: (0, i))
+    out = jax.ShapeDtypeStruct((units, width), jnp.float32)
+    return pl.pallas_call(
+        outer_kernel,
+        grid=(width // tile,),
+        out_shape=(out, out, out),
+        in_specs=[whole, whole, whole, tall, tall],
+        out_specs=[flat, flat, flat],
+        scratch_shapes=[pltpu.VMEM((3, units, rows), jnp.bfloat16)],
+        cost_estimate=pl.CostEstimate(
+            flops=6 * rows * units * width,
+            bytes_accessed=4 * rows * width + 12 * units * width,
+            transcendentals=0,
+        ),
+        name="weight_grads",
+    )(hidden, back_gate, back_up, state, cot)
+
+
+def conv_forward(conv_outer, conv_inner, conv_input, conv_taps):
+    tok_count = conv_inner.shape[1]
+    taps_count = conv_taps.shape[0]
+    rim_width = taps_count - 1
+    head_block = from_behind(
+        jnp.stack([conv_inner[:, tok_count - rim_width :], conv_input[:, tok_count - rim_width :]]),
+        "sp",
+        1,
+    )
+    inner_ext = jnp.concatenate([head_block[0], conv_inner], axis=1).astype(jnp.float32)
+    input_ext = jnp.concatenate([head_block[1], conv_input], axis=1).astype(jnp.float32)
+    inner_prod = inner_ext * input_ext
+    conv_out = jnp.zeros((conv_inner.shape[0], tok_count), jnp.float32)
+    for offset in range(taps_count):
+        conv_out = (
+            conv_out + conv_taps[offset][:, None] * inner_prod[:, offset : offset + tok_count]
+        )
+    outer_f = conv_outer.astype(jnp.float32)
+    mixer_act = (outer_f * conv_out).astype(jnp.bfloat16)
+    return conv_out, outer_f, mixer_act
+
+
+def conv_backward(back_mixer, conv_out, outer_f, conv_inner, conv_input, conv_taps):
+    tok_count = conv_inner.shape[1]
+    taps_count = conv_taps.shape[0]
+    rim_width = taps_count - 1
+    grad_outer = (back_mixer * conv_out).astype(jnp.bfloat16)
+    back_conv = back_mixer * outer_f
+    tail_back = from_behind(back_conv[:, :rim_width], "sp", -1)
+    back_ext = jnp.concatenate([back_conv, tail_back], axis=1)
+    back_prod = jnp.zeros_like(back_conv)
+    for offset in range(taps_count):
+        shift_by = rim_width - offset
+        back_prod = (
+            back_prod + conv_taps[offset][:, None] * back_ext[:, shift_by : shift_by + tok_count]
+        )
+    grad_inner = (back_prod * conv_input.astype(jnp.float32)).astype(jnp.bfloat16)
+    grad_input = (back_prod * conv_inner.astype(jnp.float32)).astype(jnp.bfloat16)
+    return grad_outer, grad_inner, grad_input
+
+
+def whole_rows(
+    conv_outer,
+    conv_inner,
+    conv_input,
+    conv_taps,
+    out_proj,
+    mixed_state,
+    route_ids,
+    route_weights,
+    w_gate,
+    w_up,
+    w_down,
+    cotangent,
+):
+    experts = w_gate.shape[0] * lax.axis_size("sp")
+    gate_w, up_w, down_w = w_gate[0], w_up[0], w_down[0]
+    choice = route_ids[:, :, None] == jnp.arange(experts, dtype=jnp.int32)[None, None, :]
+    scale_of = jnp.sum(jnp.where(choice, route_weights[:, :, None], 0.0), axis=1).T
+    scales = lax.all_to_all(
+        scale_of[:, None], "sp", split_axis=0, concat_axis=1, tiled=True
+    ).reshape(-1, 1)
+    conv_out, outer_f, mixer_act = conv_forward(conv_outer, conv_inner, conv_input, conv_taps)
+    cot_all, rows_in = gather_all(cotangent, mixed_state)
+    gate_pre = jnp.einsum("rd,fd->rf", rows_in, gate_w, preferred_element_type=jnp.float32)
+    up_pre = jnp.einsum("rd,fd->rf", rows_in, up_w, preferred_element_type=jnp.float32)
+    back_hidden = scales * jnp.einsum(
+        "rd,fd->rf", cot_all, down_w, preferred_element_type=jnp.float32
+    )
+    sig_gate = jax.nn.sigmoid(gate_pre)
+    silu_gate = gate_pre * sig_gate
+    hidden = (scales * (silu_gate * up_pre)).astype(jnp.bfloat16)
+    back_gate = (back_hidden * up_pre * sig_gate * (1.0 + gate_pre * (1.0 - sig_gate))).astype(
+        jnp.bfloat16
+    )
+    back_up = (back_hidden * silu_gate).astype(jnp.bfloat16)
+    grad_mixed, tokens, quarter, act_all = reduce_all(
+        jnp.concatenate([back_gate, back_up], axis=1), gate_w, up_w, cotangent, mixer_act
+    )
+    back_mixer = jnp.einsum("cd,td->ct", out_proj, tokens, preferred_element_type=jnp.float32)
+    grad_proj = jnp.dot(act_all, quarter, preferred_element_type=jnp.float32)
+    grad_gate_e, grad_up_e, grad_down_e = weight_grads(
+        hidden, back_gate, back_up, rows_in, cot_all
+    )
+    grad_outer, grad_inner, grad_input = conv_backward(
+        back_mixer, conv_out, outer_f, conv_inner, conv_input, conv_taps
+    )
+    return (
+        grad_gate_e[None],
+        grad_up_e[None],
+        grad_down_e[None],
+        grad_mixed,
+        grad_proj,
+        grad_outer,
+        grad_inner,
+        grad_input,
+    )
+
+
+def routed_rows(
     conv_outer,
     conv_inner,
     conv_input,
@@ -264,99 +818,52 @@
     local_experts = w_gate.shape[0]
     experts = local_experts * sp_size
     capacity = 4 * tok_count // experts
-    if capacity == tok_count and sp_size == 4 and lax.axis_size("tp") % 2 == 0:
-        choice = route_ids[:, :, None] == jnp.arange(experts, dtype=jnp.int32)[None, None, :]
-        scale_of = jnp.sum(jnp.where(choice, route_weights[:, :, None], 0.0), axis=1).T
-        scales = lax.all_to_all(
-            scale_of[:, None], "sp", split_axis=0, concat_axis=1, tiled=True
-        ).reshape(-1, 1)
-        cot_all, rows_in = gather_all(cotangent, mixed_state)
-        rows_grad = (cot_all.astype(jnp.float32) * scales).astype(jnp.bfloat16)
-        partial_value, grad_gate_e, grad_up_e, grad_down_e = expert_step(
-            rows_in, rows_grad, w_gate[0], w_up[0], w_down[0]
-        )
-        tall = lax.psum_scatter(
-            partial_value, "tp", scatter_dimension=1, tiled=True
-        )
-        tall, grad_gate_e, grad_up_e, grad_down_e = lax.optimization_barrier(
-            (tall, grad_gate_e, grad_up_e, grad_down_e)
-        )
-        summed = sum_blocks(tall, sp_size, tok_count, col_count)
-        grad_mixed = (cotangent.astype(jnp.float32) + summed).astype(jnp.bfloat16)
-    else:
-        flat_ids = route_ids.reshape(-1)
-        onehot = (flat_ids[:, None] == jnp.arange(experts, dtype=jnp.int32)[None, :]).astype(jnp.int32)
-        slot_pos = jnp.sum(jnp.cumsum(onehot, axis=0) * onehot, axis=1) - 1
-        slot_dest = flat_ids * capacity + slot_pos
-        token_of = jnp.arange(flat_ids.shape[0], dtype=jnp.int32) // top_count
-        scale_flat = route_weights.reshape(-1)[:, None]
-
-        def pack_rows(rows):
-            buffer = jnp.zeros((experts * capacity, rows.shape[1]), rows.dtype).at[slot_dest].set(rows)
-            return buffer.reshape(sp_size, local_experts, capacity, rows.shape[1])
-
-        sent_state = pack_rows(mixed_state[token_of])
-        sent_grad = pack_rows(
-            (cotangent[token_of].astype(jnp.float32) * scale_flat).astype(jnp.bfloat16)
-        )
-        recv_state, recv_grad = (
-            lax.all_to_all(sent_state, "sp", split_axis=0, concat_axis=0, tiled=True),
-            lax.all_to_all(sent_grad, "sp", split_axis=0, concat_axis=0, tiled=True),
-        )
-        state_rows, grad_rows = (
-            lax.all_gather(recv_state[:, 0], "tp", axis=2, tiled=True),
-            lax.all_gather(recv_grad[:, 0], "tp", axis=2, tiled=True),
-        )
-        width = state_rows.shape[2]
-        rows_in = state_rows.reshape(-1, width)
-        rows_grad = grad_rows.reshape(-1, width)
-        partial_value, grad_gate_e, grad_up_e, grad_down_e = expert_step(
-            rows_in, rows_grad, w_gate[0], w_up[0], w_down[0]
-        )
-        summed = lax.psum_scatter(
-            partial_value, "tp", scatter_dimension=1, tiled=True
-        )
-        back_rows = summed.reshape(sp_size, capacity, col_count)
-        arrived = lax.all_to_all(
-            back_rows[:, None], "sp", split_axis=0, concat_axis=0, tiled=True
-        ).reshape(experts * capacity, col_count)
-        picked = arrived[slot_dest].astype(jnp.float32).reshape(tok_count, top_count, col_count)
-        grad_mixed = (cotangent.astype(jnp.float32) + jnp.sum(picked, axis=1)).astype(jnp.bfloat16)
-    taps_count = conv_taps.shape[0]
-    rim_width = taps_count - 1
-    head_block = from_behind(
-        jnp.stack([conv_inner[:, tok_count - rim_width :], conv_input[:, tok_count - rim_width :]]),
-        "sp",
-        1,
-    )
-    inner_ext = jnp.concatenate([head_block[0], conv_inner], axis=1).astype(jnp.float32)
-    input_ext = jnp.concatenate([head_block[1], conv_input], axis=1).astype(jnp.float32)
-    inner_prod = inner_ext * input_ext
-    conv_out = jnp.zeros((conv_inner.shape[0], tok_count), jnp.float32)
-    for offset in range(taps_count):
-        conv_out = (
-            conv_out + conv_taps[offset][:, None] * inner_prod[:, offset : offset + tok_count]
-        )
-    outer_f = conv_outer.astype(jnp.float32)
-    mixer_act = (outer_f * conv_out).astype(jnp.bfloat16)
+    flat_ids = route_ids.reshape(-1)
+    onehot = (flat_ids[:, None] == jnp.arange(experts, dtype=jnp.int32)[None, :]).astype(jnp.int32)
+    slot_pos = jnp.sum(jnp.cumsum(onehot, axis=0) * onehot, axis=1) - 1
+    slot_dest = flat_ids * capacity + slot_pos
+    token_of = jnp.arange(flat_ids.shape[0], dtype=jnp.int32) // top_count
+    scale_flat = route_weights.reshape(-1)[:, None]
+
+    def pack_rows(rows):
+        buffer = jnp.zeros((experts * capacity, rows.shape[1]), rows.dtype).at[slot_dest].set(rows)
+        return buffer.reshape(sp_size, local_experts, capacity, rows.shape[1])
+
+    sent_state = pack_rows(mixed_state[token_of])
+    sent_grad = pack_rows(
+        (cotangent[token_of].astype(jnp.float32) * scale_flat).astype(jnp.bfloat16)
+    )
+    recv_state, recv_grad = (
+        lax.all_to_all(sent_state, "sp", split_axis=0, concat_axis=0, tiled=True),
+        lax.all_to_all(sent_grad, "sp", split_axis=0, concat_axis=0, tiled=True),
+    )
+    state_rows, grad_rows = (
+        lax.all_gather(recv_state[:, 0], "tp", axis=2, tiled=True),
+        lax.all_gather(recv_grad[:, 0], "tp", axis=2, tiled=True),
+    )
+    width = state_rows.shape[2]
+    rows_in = state_rows.reshape(-1, width)
+    rows_grad = grad_rows.reshape(-1, width)
+    partial_value, grad_gate_e, grad_up_e, grad_down_e = expert_step(
+        rows_in, rows_grad, w_gate[0], w_up[0], w_down[0]
+    )
+    summed = lax.psum_scatter(partial_value, "tp", scatter_dimension=1, tiled=True)
+    back_rows = summed.reshape(sp_size, capacity, col_count)
+    arrived = lax.all_to_all(
+        back_rows[:, None], "sp", split_axis=0, concat_axis=0, tiled=True
+    ).reshape(experts * capacity, col_count)
+    picked = arrived[slot_dest].astype(jnp.float32).reshape(tok_count, top_count, col_count)
+    grad_mixed = (cotangent.astype(jnp.float32) + jnp.sum(picked, axis=1)).astype(jnp.bfloat16)
+    conv_out, outer_f, mixer_act = conv_forward(conv_outer, conv_inner, conv_input, conv_taps)
     full_back = lax.all_gather(grad_mixed, "tp", axis=1, tiled=True)
     back_mixer = jnp.einsum("cd,td->ct", out_proj, full_back, preferred_element_type=jnp.float32)
     proj_term = jnp.dot(mixer_act, full_back, preferred_element_type=jnp.float32)
     grad_proj = lax.psum_scatter(
         proj_term.astype(jnp.bfloat16), "sp", scatter_dimension=1, tiled=True
     ).astype(jnp.float32)
-    grad_outer = (back_mixer * conv_out).astype(jnp.bfloat16)
-    back_conv = back_mixer * outer_f
-    tail_back = from_behind(back_conv[:, :rim_width], "sp", -1)
-    back_ext = jnp.concatenate([back_conv, tail_back], axis=1)
-    back_prod = jnp.zeros_like(back_conv)
-    for offset in range(taps_count):
-        shift_by = rim_width - offset
-        back_prod = (
-            back_prod + conv_taps[offset][:, None] * back_ext[:, shift_by : shift_by + tok_count]
-        )
-    grad_inner = (back_prod * conv_input.astype(jnp.float32)).astype(jnp.bfloat16)
-    grad_input = (back_prod * conv_inner.astype(jnp.float32)).astype(jnp.bfloat16)
+    grad_outer, grad_inner, grad_input = conv_backward(
+        back_mixer, conv_out, outer_f, conv_inner, conv_input, conv_taps
+    )
     return (
         grad_gate_e[None],
         grad_up_e[None],
@@ -367,6 +874,15 @@
         grad_inner,
         grad_input,
     )
+
+
+def shards(*operands):
+    mixed_state, cotangent, w_gate = operands[5], operands[11], operands[8]
+    tok_count = mixed_state.shape[0]
+    sp_size, tp_size = lax.axis_size("sp"), lax.axis_size("tp")
+    capacity = 4 * tok_count // (w_gate.shape[0] * sp_size)
+    small = capacity == tok_count and sp_size == 4 and tp_size == 8
+    return (whole_rows if small else routed_rows)(*operands)
 
 
 def solution(mesh):

time: 301 us -> 210 us (0.70)
  waiting for transfers between devices: 126 us -> 1.5 us
  Pallas kernels: 84.9 us -> 170 us
  matrix products: 43.1 us -> 19.4 us
  blocking collectives: 13.6 us -> 0 us
  between operations: 14 us -> 0.86 us
    reduce_scatter x2 -> x0, waiting for transfers between devices: 95.2 us -> none  [the longest x1 66.5 us: shards(): lax.psum_scatter(partial_value, 'tp', scatter_dimension=1, tiled=True)]
    pallas_call x1 -> x2, Pallas kernels: 10.3 us -> 92.4 us  [the longest x1 76.4 us: reduce_all(): pl.pallas_call(reduce_kernel, out_shape=(jax.ShapeDtypeStruct((rows, half...]
    all_gather x1 -> x0, waiting for transfers between devices: 28.2 us -> none  [shards(): full_back = lax.all_gather(grad_mixed, 'tp', axis=1, tiled=True)]
    dot_general x8 -> x5, matrix products: 43.1 us -> 19.4 us  [the longest x1 7.1 us: whole_rows(): jnp.einsum('rd,fd->rf', cot_all, down_w, preferred_element_type=jnp.float32)]
    all_to_all x1 -> x0, blocking collectives: 13.6 us -> none  [sum_blocks(): lax.all_to_all(tall.reshape(sp_size, 1, rows, cols), 'sp', split_axis=0,...]
  transfers between devices with their start and end apart: 6 -> 3, of which waited for: 4 -> 1; matrix products, arithmetic and copies ran while one was open for 11% -> 7% of each run, Pallas kernels for 25% -> 37%
where the time goes in v1:
time: 210 us; the launch traced here: 207 us
  Pallas kernels  170 us (81%)
  matrix products  19.4 us (9%)
  starting transfers between devices  6.35 us (3%)
  local copies, waits for them, and re-layouts  5.17 us (2%)
  other arithmetic  4.57 us (2%)
    pallas_call x1, Pallas kernels, gather_all(): pl.pallas_call(functools.partial(gather_kernel, levels), out_shape=(whole...  77.1 us
    pallas_call x1, Pallas kernels, reduce_all(): pl.pallas_call(reduce_kernel, out_shape=(jax.ShapeDtypeStruct((rows, half...  76.4 us
    pallas_call x1, Pallas kernels, weight_grads(): pl.pallas_call(outer_kernel, grid=(width // tile,), out_shape=(out, out,...  16 us
    dot_general x1, matrix products, whole_rows(): jnp.einsum('rd,fd->rf', cot_all, down_w, preferred_element_type=jnp.float32)  7.1 us
    dot_general x1, matrix products, whole_rows(): jnp.einsum('rd,fd->rf', rows_in, gate_w, preferred_element_type=jnp.float32)  6.5 us
  transfers between devices with their start and end apart: 3, of which 1 were waited for; matrix products, arithmetic and copies ran while one was open for 7% of the time, Pallas kernels for 37%

profile of v1, /device:TPU:7, one launch (start us, length us, event | category | flops | bytes accessed | tf_op | source)
XLA Modules:
  0.0 207.4 jit_solution(13048040049875821695)
XLA Ops:
  0.6 0.0 copy-start
  0.6 0.9 select_reduce_fusion
  1.5 0.6 copy.50
  2.1 3.6 %all-to-all-start = ((f32[4,1,256]{2,1,0:T(1,128)}), f32[4,1,256]{2,1,0:T(1,128)S(1)}, u32[]{:S(2)}, u32[]{:S(2)}) async-start(f32[4,1,256]{2,1,0:T(1,128)} %copy.50), calls=%async_computation | async-start | bytes 8192 | tf_op jit(solution)/shard_map/all_to_all | solution.py:760
  5.7 0.9 slice.44
  6.7 0.1 copy.66
  6.8 0.9 slice.43
  7.7 0.1 copy.65
  7.8 0.2 copy.59
  8.0 1.3 collective-permute-start
  9.3 77.1 %gather_all.1 = (bf16[1024,4096]{1,0:T(8,128)(2,1)}, bf16[1024,4096]{1,0:T(8,128)(2,1)}) custom-call(bf16[256,512]{1,0:T(8,128)(2,1)} %cot_in.3, bf16[256,512]{1,0:T(8,128)(2,1)} %state_in.1), custom_call_target="tpu_custom_call" | custom-call | tf_op jit(solution)/shard_map/gather_all/pallas_call | solution.py:224
  86.5 0.0 copy-start.4
  86.5 0.0 copy-start.15
  86.5 6.5 %fusion.16 = f32[1024,256]{1,0:T(8,128)S(1)} fusion(bf16[1024,4096]{1,0:T(8,128)(2,1)} %get-tuple-element.17.state_ref, bf16[1,256,4096]{2,1,0:T(8,128)(2,1)} %param.20), kind=kOutput, calls=%fused_computation.37 | convolution fusion | flops 2147483648 | bytes 11534336 | tf_op jit(solution)/shard_map/rd,fd->rf/dot_general | solution.py:765
  93.0 0.0 copy-done.4
  93.0 0.5 copy-done.15
  93.5 3.4 %fusion.14 = f32[1024,256]{1,0:T(8,128)} fusion(bf16[1024,4096]{1,0:T(8,128)(2,1)S(1)} %copy-done.15, bf16[1,256,4096]{2,1,0:T(8,128)(2,1)S(1)} %copy-done.4), kind=kOutput, calls=%fused_computation.35 | convolution fusion | flops 2147483648 | bytes 11534336 | tf_op jit(solution)/shard_map/rd,fd->rf/dot_general | solution.py:766
  96.9 0.0 copy-done.14
  96.9 0.0 collective-permute-done
  96.9 0.0 copy-done.6
  97.0 0.0 copy-done.8
  97.0 0.2 convert_multiply_fusion
  97.2 0.0 copy-done.12
  97.2 1.0 fusion.6
  98.2 0.0 all-to-all-done
  98.2 0.0 copy-done
  98.2 7.1 %multiply_convert_fusion = (bf16[1024,256]{1,0:T(8,128)(2,1)S(1)}, bf16[1024,256]{1,0:T(8,128)(2,1)S(1)}, bf16[1024,256]{1,0:T(8,128)(2,1)}) fusion(f32[1024,256]{1,0:T(8,128)S(1)} %fusion.16, f32[1024,256]{1,0:T(8,128)} %fusion.14, f32[1024]{0:T(1024)S(1)} %bitcast.49, bf16[1024,4096]{1,0:T(8,128)(2,1)} %get-tuple-element.18.cot_ref, ...), kind=kOutput, calls=%fused_computation.5 | convolution fusion | flops 2151940096 | bytes 14159872 | tf_op jit(solution)/shard_map/rd,fd->rf/dot_general | solution.py:767
  105.3 0.1 pad_maximum_fusion.back_in
  105.4 0.7 copy-done.10
  106.1 0.2 copy-done.11
  106.2 16.0 %weight_grads.1 = (f32[256,4096]{1,0:T(8,128)}, f32[256,4096]{1,0:T(8,128)}, f32[256,4096]{1,0:T(8,128)}) custom-call(bf16[1024,256]{1,0:T(8,128)(2,1)} %get-tuple-element.32.hidden_ref, bf16[1024,256]{1,0:T(8,128)(2,1)} %copy-done.11, bf16[1024,256]{1,0:T(8,128)(2,1)} %copy-done.10, bf16[1024,4096]{1,0:T(8,128)(2,1)} %get-tuple-element.17.state_ref, ...), custom_call_target="tpu_custom_call" | custom-call | flops 6442450944 | bytes 29360128 | tf_op jit(solution)/shard_map/weight_grads/pallas_call | solution.py:685
  122.2 0.0 copy-done.1
  122.2 76.4 %reduce_all.1 = (bf16[256,512]{1,0:T(8,128)(2,1)S(1)}, bf16[256,4096]{1,0:T(8,128)(2,1)S(1)}, bf16[1024,1024]{1,0:T(8,128)(2,1)}, bf16[256,1024]{1,0:T(8,128)(2,1)S(1)}) custom-call(bf16[1024,512]{1,0:T(8,128)(2,1)S(1)} %pad_maximum_fusion.back_in, bf16[256,4096]{1,0:T(8,128)(2,1)} %bitcast.38, bf16[256,4096]{1,0:T(8,128)(2,1)} %bitcast.39, ...), custom_call_target="tpu_custom_call" | custom-call | tf_op jit(solution)/shard_map/reduce_all/pallas_call | solution.py:620
  198.7 0.0 copy-start.5
  198.7 0.0 copy-start.13
  198.7 0.0 copy-start.2
  198.7 0.7 convolution_bitcast_fusion
  199.5 0.2 copy-done.5
  199.6 0.0 copy-done.13
  199.7 0.7 convert_multiply_fusion.1
  200.4 1.4 collective-permute-start.1
  201.8 0.0 copy-start.9
  201.8 1.7 fusion.21
  203.5 1.5 collective-permute-done.1
  205.0 0.0 copy-done.7
  205.0 1.0 multiply_convert_fusion.3
  206.0 0.7 multiply_convert_fusion.4
  206.7 0.7 copy.68
  (16 shorter events, 0.1 us)
Async XLA Ops:
  0.6 97.6 %copy-start = (bf16[1,256,4096]{2,1,0:T(8,128)(2,1)S(1)}, bf16[1,256,4096]{2,1,0:T(8,128)(2,1)}, u32[]{:S(2)}) copy-start(bf16[1,256,4096]{2,1,0:T(8,128)(2,1)} %param.22) | copy-start | bytes 6291460
  2.1 96.1 %all-to-all-start = ((f32[4,1,256]{2,1,0:T(1,128)}), f32[4,1,256]{2,1,0:T(1,128)S(1)}, u32[]{:S(2)}, u32[]{:S(2)}) async-start(f32[4,1,256]{2,1,0:T(1,128)} %copy.50), calls=%async_computation | async-start | bytes 8192 | tf_op jit(solution)/shard_map/all_to_all | solution.py:760
  8.0 88.9 %collective-permute-start = (bf16[2,256,2]{2,1,0:T(8,128)(2,1)S(1)}, bf16[2,256,2]{2,1,0:T(8,128)(2,1)S(1)}, u32[]{:S(2)}, u32[]{:S(2)}) collective-permute-start(bf16[2,256,2]{2,1,0:T(8,128)(2,1)S(1)} %copy.59), channel_id=1, source_target_pairs={{0,8},{8,16},{16,24},{1,9},{9,17},{17,25},{2,10},{10,18},{18,26},{... | collective-permute-start | bytes 6152 | tf_op jit(solution)/shard_map/ppermute | solution.py:14
  86.5 6.5 %copy-start.4 = (bf16[1,256,4096]{2,1,0:T(8,128)(2,1)S(1)}, bf16[1,256,4096]{2,1,0:T(8,128)(2,1)}, u32[]{:S(2)}) copy-start(bf16[1,256,4096]{2,1,0:T(8,128)(2,1)} %param.21) | copy-start | bytes 6291460
  86.5 7.0 %copy-start.15 = (bf16[1024,4096]{1,0:T(8,128)(2,1)S(1)}, bf16[1024,4096]{1,0:T(8,128)(2,1)}, u32[]{:S(2)}) copy-start(bf16[1024,4096]{1,0:T(8,128)(2,1)} %get-tuple-element.17.state_ref) | copy-start | bytes 25165828
  93.5 3.4 %copy-start.14 = (f32[3,256]{1,0:T(4,128)S(1)}, f32[3,256]{1,0:T(4,128)}, u32[]{:S(2)}) copy-start(f32[3,256]{1,0:T(4,128)} %param.15) | copy-start | bytes 9220
  93.5 3.5 %copy-start.6 = (bf16[256,256]{1,0:T(8,128)(2,1)S(1)}, bf16[256,256]{1,0:T(8,128)(2,1)}, u32[]{:S(2)}) copy-start(bf16[256,256]{1,0:T(8,128)(2,1)} %param.13) | copy-start | bytes 393220
  93.5 3.5 %copy-start.8 = (bf16[256,256]{1,0:T(8,128)(2,1)S(1)}, bf16[256,256]{1,0:T(8,128)(2,1)}, u32[]{:S(2)}) copy-start(bf16[256,256]{1,0:T(8,128)(2,1)} %param.14) | copy-start | bytes 393220
  93.5 3.7 %copy-start.12 = (bf16[256,256]{1,0:T(8,128)(2,1)S(1)}, bf16[256,256]{1,0:T(8,128)(2,1)}, u32[]{:S(2)}) copy-start(bf16[256,256]{1,0:T(8,128)(2,1)} %param.12) | copy-start | bytes 393220
  105.3 0.8 copy-start.10
  105.3 1.0 copy-start.11
  106.2 16.0 %copy-start.1 = (bf16[256,512]{1,0:T(8,128)(2,1)S(1)}, bf16[256,512]{1,0:T(8,128)(2,1)}, u32[]{:S(2)}) copy-start(bf16[256,512]{1,0:T(8,128)(2,1)} %cot_in.3) | copy-start | bytes 786436
  122.2 76.4 %copy-start.3 = (bf16[256,4096]{1,0:T(8,128)(2,1)S(1)}, bf16[256,4096]{1,0:T(8,128)(2,1)}, u32[]{:S(2)}) copy-start(bf16[256,4096]{1,0:T(8,128)(2,1)} %param.16) | copy-start | bytes 6291460
  198.7 1.0 copy-start.5
  198.7 1.0 copy-start.13
  198.7 3.1 %copy-start.2 = (bf16[1024,1024]{1,0:T(8,128)(2,1)S(1)}, bf16[1024,1024]{1,0:T(8,128)(2,1)}, u32[]{:S(2)}) copy-start(bf16[1024,1024]{1,0:T(8,128)(2,1)} %get-tuple-element.24) | copy-start | bytes 6291460
  200.4 4.7 %copy-start.7 = (bf16[256,256]{1,0:T(8,128)(2,1)S(1)}, bf16[256,256]{1,0:T(8,128)(2,1)}, u32[]{:S(2)}) copy-start(bf16[256,256]{1,0:T(8,128)(2,1)} %param.13) | copy-start | bytes 393220
  200.4 4.6 %collective-permute-start.1 = (f32[256,2]{1,0:T(8,128)S(1)}, f32[256,2]{1,0:T(8,128)S(1)}, u32[]{:S(2)}, u32[]{:S(2)}) collective-permute-start(f32[256,2]{1,0:T(8,128)S(1)} %slice.60), channel_id=1, source_target_pairs={{8,0},{16,8},{24,16},{9,1},{17,9},{25,17},{10,2},{18,10},{26,18},{... | collective-permute-start | bytes 6152 | tf_op jit(solution)/shard_map/ppermute | solution.py:14
  201.8 4.2 %copy-start.9 = (bf16[256,256]{1,0:T(8,128)(2,1)S(1)}, bf16[256,256]{1,0:T(8,128)(2,1)}, u32[]{:S(2)}) copy-start(bf16[256,256]{1,0:T(8,128)(2,1)} %param.14) | copy-start | bytes 393220

commit v2 on v1

--- a/solution.py
+++ b/solution.py
@@ -59,12 +59,63 @@
     return (partial_value, grad_gate_e, grad_up_e, grad_down_e)
 
 
-Z_UP, Z_DOWN, BY_X, BY_Y, HALF_X, HALF_Y, PEER = range(7)
+COLUMN, BY_X, BY_Y, CORNER, Z_CORNER, PRODUCT = range(6)
+FAR, NEAR, IN_X, IN_Y, HALF_X, HALF_Y, IN_CORNER, PEER = range(8)
 KINDS = PEER + 4
-
-
-def gather_kernel(levels, cot_in, state_in, cot_out, state_out, own_sem, send_sem, recv_sem):
+LEVELS = 4
+END_ORDER = (
+    (0, 1, 0), (0, 0, 0), (1, 1, 0), (2, 1, 0), (0, 1, 1), (1, 0, 0),
+    (2, 0, 0), (0, 0, 1), (3, 1, 0), (5, 1, 0), (0, 1, 2), (1, 1, 1),
+    (2, 1, 1), (3, 0, 0), (0, 0, 2), (5, 0, 0), (1, 0, 1), (2, 0, 1),
+    (0, 1, 3), (1, 1, 2), (2, 1, 2), (4, 1, 1), (5, 1, 1), (1, 0, 2),
+    (2, 0, 2), (0, 0, 3), (1, 1, 3), (2, 1, 3), (4, 0, 1), (3, 1, 2),
+    (5, 0, 1), (5, 1, 2), (4, 1, 3), (3, 0, 2), (5, 1, 3), (5, 0, 2),
+    (1, 0, 3), (2, 0, 3), (4, 0, 3), (5, 0, 3),
+)
+INNER_ORDER = (
+    (0, 1, 1), (0, 0, 1), (0, 1, 0), (1, 1, 1), (2, 1, 1), (0, 1, 2),
+    (0, 0, 0), (1, 0, 1), (2, 0, 1), (0, 0, 2), (1, 1, 0), (2, 1, 0),
+    (0, 1, 3), (3, 1, 1), (5, 1, 1), (4, 1, 0), (0, 0, 3), (5, 1, 0),
+    (1, 1, 2), (2, 1, 2), (4, 0, 0), (1, 0, 0), (2, 0, 0), (5, 0, 0),
+    (3, 0, 1), (4, 1, 3), (5, 0, 1), (1, 0, 2), (2, 0, 2), (4, 0, 3),
+    (1, 1, 3), (2, 1, 3), (5, 1, 3), (1, 0, 3), (2, 0, 3), (5, 0, 3),
+    (3, 1, 2), (5, 1, 2), (3, 0, 2), (5, 0, 2),
+)
+
+
+def gather_kernel(
+    cot_in,
+    state_in,
+    scale_in,
+    inner_in,
+    input_in,
+    gate_in,
+    up_in,
+    down_in,
+    cot_out,
+    state_out,
+    hidden_out,
+    back_out,
+    head_out,
+    cot_rows,
+    state_rows,
+    gate_w,
+    up_w,
+    down_w,
+    gate_acc,
+    up_acc,
+    back_acc,
+    scale_land,
+    own_sem,
+    weight_sem,
+    store_sem,
+    small_send,
+    small_recv,
+    send_sem,
+    recv_sem,
+):
     sp, tp = lax.axis_index("sp"), lax.axis_index("tp")
+    levels = LEVELS
     level, core = tp // 2, tp % 2
     beside_x = sp + 1 - 2 * (sp % 2)
     beside_y = (sp + 2) % 4
@@ -72,7 +123,8 @@
     peer = tp + 1 - 2 * core
     rows, cols = cot_in.shape
     half = rows // 2
-    ins, outs = (cot_in, state_in), (cot_out, state_out)
+    ins, outs, stores = (cot_in, state_in), (cot_rows, state_rows), (cot_out, state_out)
+    at_end = (level == 0) | (level == levels - 1)
 
     barrier = pltpu.get_barrier_semaphore()
 
@@ -86,15 +138,19 @@
 
     greet(beside_x, tp)
     greet(beside_y, tp)
+    greet(across, tp)
     greet(sp, peer)
     pl.when(level > 0)(lambda: greet(sp, tp - 2))
     pl.when(level < levels - 1)(lambda: greet(sp, tp + 2))
-    one = jnp.int32(1)
-    none = jnp.int32(0)
-    pl.semaphore_wait(
-        barrier,
-        3 + jnp.where(level > 0, one, none) + jnp.where(level < levels - 1, one, none),
-    )
+    weight_copies = [
+        pltpu.make_async_copy(source, target, weight_sem.at[at])
+        for at, (source, target) in enumerate(
+            ((gate_in, gate_w), (up_in, up_w), (down_in, down_w))
+        )
+    ]
+    for copy in weight_copies:
+        copy.start()
+    pl.semaphore_wait(barrier, 6 - jnp.where(at_end, jnp.int32(1), jnp.int32(0)))
 
     def block(array, of_sp, of_level, of_core, start=0, size=rows):
         return outs[array].at[
@@ -102,138 +158,282 @@
             pl.ds(pl.multiple_of((of_level * 2 + of_core) * cols, 128), cols),
         ]
 
-    def remote(array, kind, of_level, source, target, to_sp, to_tp):
+    def copy_to(source, target, send, recv, to_sp, to_tp):
         return pltpu.make_async_remote_copy(
             src_ref=source,
             dst_ref=target,
-            send_sem=send_sem.at[array, kind, of_level],
-            recv_sem=recv_sem.at[array, kind, of_level],
+            send_sem=send,
+            recv_sem=recv,
             device_id=(to_sp, to_tp),
             device_id_type=pl.DeviceIdType.MESH,
         )
 
-    def spread(array, of_level, source, kind, to_sp, to_tp):
-        remote(
-            array, kind, of_level, source, block(array, sp, of_level, core), to_sp, to_tp
-        ).start()
-
-    def pieces(array, of_level):
-        return {
-            Z_UP: block(array, sp, of_level, core),
-            Z_DOWN: block(array, sp, of_level, core),
-            BY_X: block(array, beside_x, of_level, core),
-            BY_Y: block(array, beside_y, of_level, core),
-            HALF_Y: block(array, across, of_level, core, 0, half),
-            HALF_X: block(array, across, of_level, core, half, half),
-            PEER: block(array, sp, of_level, 1 - core),
-            PEER + 1: block(array, beside_x, of_level, 1 - core),
-            PEER + 2: block(array, beside_y, of_level, 1 - core),
-            PEER + 3: block(array, across, of_level, 1 - core),
-        }
-
-    def arrive(array, kind, of_level):
-        piece = pieces(array, of_level)[kind]
+    def remote(array, kind, of_level, source, target, to_sp, to_tp, lands=None):
+        return copy_to(
+            source,
+            target,
+            send_sem.at[array, kind, of_level],
+            recv_sem.at[array, kind if lands is None else lands, of_level],
+            to_sp,
+            to_tp,
+        )
+
+    def scale_copy(at, to_sp):
+        return copy_to(
+            scale_in.at[to_sp],
+            scale_land.at[sp],
+            small_send.at[at],
+            small_recv.at[sp],
+            to_sp,
+            tp,
+        )
+
+    def head_copy(which):
+        source = (inner_in, input_in)[which]
+        width = source.shape[1]
+        return copy_to(
+            source.at[:, pl.ds(width - 128, 128)],
+            head_out.at[which],
+            small_send.at[3 + which],
+            small_recv.at[4 + which],
+            sp + 1,
+            tp,
+        )
+
+    others = (beside_x, beside_y, across)
+    for at, to_sp in enumerate(others):
+        scale_copy(at, to_sp).start()
+    scale_land[sp] = scale_in[sp]
+
+    def pass_on(sent, *operands, lands=None):
+        def build():
+            return remote(*operands, lands=lands)
+
+        build().start()
+        sent.append(build)
+
+    def arrive(array, kind, of_level, of_sp, of_core, start=0, size=rows):
+        piece = block(array, of_sp, of_level, of_core, start, size)
         remote(array, kind, of_level, piece, piece, sp, peer).wait_recv()
 
-    def left(array, kind, of_level):
-        piece = pieces(array, of_level)[kind]
-        remote(array, kind, of_level, piece, piece, sp, peer).wait_send()
-
-    def hand_on(array, of_level, kind, of_sp, to_sp, to_tp, start=0, size=rows):
-        piece = block(array, of_sp, of_level, core, start, size)
-        remote(array, kind, of_level, piece, piece, to_sp, to_tp).start()
-
-    def column(array, step, up):
-        of_level = level if step == 0 else (level - step if up else level + step)
-        if step == 0:
-            source = ins[array]
+    def inward(array, place, inner, sent):
+        of_level = jnp.where(level < levels // 2, place, levels - 1 - place)
+        far = tp + jnp.where(level < levels // 2, 2, -2)
+        near = 2 * tp - far
+        flat = place in ((1, 2) if inner else (0, 2))
+        mine = place == inner
+
+        def hand_on(kind, of_sp, to_sp, to_tp, start=0, size=rows, lands=None):
+            piece = block(array, of_sp, of_level, core, start, size)
+            pass_on(sent, array, kind, of_level, piece, piece, to_sp, to_tp, lands=lands)
+
+        def column():
+            target = block(array, sp, of_level, core)
+            source = ins[array] if mine else target
+            if mine:
+                pltpu.make_async_copy(source, target, own_sem.at[array]).start()
+            else:
+                arrive(array, FAR, of_level, sp, core)
+
+            def give(kind, to_sp, to_tp, lands=None):
+                pass_on(sent, array, kind, of_level, source, target, to_sp, to_tp, lands=lands)
+
+            if place <= inner:
+                give(FAR, sp, far)
+            if inner and place >= inner:
+                give(NEAR, sp, near, FAR)
+            give(IN_X, beside_x, tp)
+            give(IN_Y, beside_y, tp)
+            give(PEER, sp, peer)
+
+        def by_x():
+            arrive(array, IN_X, of_level, beside_x, core)
+            if flat:
+                hand_on(HALF_Y, beside_x, beside_y, tp, 0, half)
+            hand_on(PEER + 1, beside_x, sp, peer)
+
+        def by_y():
+            arrive(array, IN_Y, of_level, beside_y, core)
+            if flat:
+                hand_on(HALF_X, beside_y, beside_x, tp, half, half)
+            hand_on(PEER + 2, beside_y, sp, peer)
+
+        def corner():
+            if flat:
+                arrive(array, HALF_X, of_level, across, core, half, half)
+                arrive(array, HALF_Y, of_level, across, core, 0, half)
+            else:
+                arrive(array, IN_CORNER, of_level, across, core)
+            if place == 0:
+                hand_on(IN_CORNER, across, sp, far)
+            elif inner and place in (1, 3):
+                hand_on(IN_CORNER, across, sp, near)
+            hand_on(PEER + 3, across, sp, peer)
+
+        return of_level, mine, (column, by_x, by_y, corner, corner)
+
+    def slab(ref, of_level):
+        return ref.at[:, pl.ds(pl.multiple_of(of_level * 2 * cols, 128), 2 * cols)]
+
+    def store(array, of_level):
+        return pltpu.make_async_copy(
+            slab(outs[array], of_level),
+            slab(stores[array], of_level),
+            store_sem.at[array, of_level],
+        )
+
+    def product(array, of_level, mine, first):
+        for at, of_sp in enumerate((sp, beside_x, beside_y, across)):
+            arrive(array, PEER + at, of_level, of_sp, 1 - core)
+        if mine:
             pltpu.make_async_copy(
-                source, block(array, sp, level, core), own_sem.at[array]
-            ).start()
-        else:
-            arrive(array, Z_UP if up else Z_DOWN, of_level)
-            source = block(array, sp, of_level, core)
-        if step == 0 or up:
-            pl.when(level < levels - 1)(
-                lambda: spread(array, of_level, source, Z_UP, sp, tp + 2)
-            )
-        if step == 0 or not up:
-            pl.when(level > 0)(lambda: spread(array, of_level, source, Z_DOWN, sp, tp - 2))
-        spread(array, of_level, source, BY_X, beside_x, tp)
-        spread(array, of_level, source, BY_Y, beside_y, tp)
-        spread(array, of_level, source, PEER, sp, peer)
-
-    def plane(array, step, up):
-        of_level = level - step if up else level + step
-        arrive(array, BY_X, of_level)
-        hand_on(array, of_level, HALF_Y, beside_x, beside_y, tp, 0, half)
-        hand_on(array, of_level, PEER + 1, beside_x, sp, peer)
-        arrive(array, BY_Y, of_level)
-        hand_on(array, of_level, HALF_X, beside_y, beside_x, tp, half, half)
-        hand_on(array, of_level, PEER + 2, beside_y, sp, peer)
-
-    def corner(array, step, up):
-        of_level = level - step if up else level + step
-        arrive(array, HALF_X, of_level)
-        arrive(array, HALF_Y, of_level)
-        hand_on(array, of_level, PEER + 3, across, sp, peer)
-
-    def each(action, step):
-        if not 0 <= step < levels:
-            return
-        if step == 0:
-            for array in range(2):
-                action(array, 0, True)
-            return
-
-        @pl.when(level >= step)
-        def _():
-            for array in range(2):
-                action(array, step, True)
-
-        @pl.when(level < levels - step)
-        def _():
-            for array in range(2):
-                action(array, step, False)
-
-    for step in range(levels + 2):
-        each(column, step)
-        each(plane, step - 1)
-        each(corner, step - 2)
-
+                ins[array], block(array, sp, level, core), own_sem.at[array]
+            ).wait()
+        if first:
+            for at in (0, 1) if array == 1 else (2,):
+                weight_copies[at].wait()
+        store(array, of_level).start()
+        pairs = ((gate_w, gate_acc), (up_w, up_acc)) if array == 1 else ((down_w, back_acc),)
+        span = pl.ds(pl.multiple_of(of_level * 2 * cols, 128), 2 * cols)
+
+        def one(at, _):
+            lines = pl.ds(pl.multiple_of(at * rows, 128), rows)
+            for weight, acc in pairs:
+                value = lax.dot_general(
+                    outs[array][lines, span],
+                    weight[:, span],
+                    (((1,), (1,)), ((), ())),
+                    preferred_element_type=jnp.float32,
+                )
+                acc[lines, :] = value if first else acc[lines, :] + value
+            return 0
+
+        lax.fori_loop(0, 4, one, 0)
+
+    def give_head():
+        head_copy(0).start()
+        head_copy(1).start()
+
+    def follow(order, inner):
+        sent, begun = [], set()
+        flats = (1, 2) if inner else (0, 2)
+        last = max(
+            at
+            for at, (kind, _, place) in enumerate(order)
+            if kind == COLUMN or (kind in (BY_X, BY_Y) and place in flats)
+        )
+        for at, (kind, array, place) in enumerate(order):
+            if at == last + 1:
+                pl.when(sp < 3)(give_head)
+            of_level, mine, actions = inward(array, place, inner, sent)
+            if kind == PRODUCT:
+                product(array, of_level, mine, array not in begun)
+                begun.add(array)
+            else:
+                actions[kind]()
+        for build in sent:
+            build().wait_send()
+
+    pl.when(at_end)(lambda: follow(END_ORDER, 0))
+    pl.when(jnp.logical_not(at_end))(lambda: follow(INNER_ORDER, 1))
+
+    for at, to_sp in enumerate(others):
+        copy_to(
+            scale_land.at[to_sp],
+            scale_land.at[to_sp],
+            small_send.at[at],
+            small_recv.at[to_sp],
+            sp,
+            peer,
+        ).wait_recv()
+    units = hidden_out.shape[1]
+
+    def finish(at, _):
+        lines = pl.ds(pl.multiple_of(at * rows, 128), rows)
+        scale = jnp.broadcast_to(scale_land[at, 0:1, :], (units, rows)).T
+        gate_pre, up_pre = gate_acc[lines, :], up_acc[lines, :]
+        sig_gate = 1.0 / (1.0 + jnp.exp(-gate_pre))
+        silu_gate = gate_pre * sig_gate
+        back_hidden = scale * back_acc[lines, :]
+        hidden_out[lines, :] = (scale * (silu_gate * up_pre)).astype(hidden_out.dtype)
+        back_out[lines, :units] = (
+            back_hidden * up_pre * sig_gate * (1.0 + gate_pre * (1.0 - sig_gate))
+        ).astype(back_out.dtype)
+        back_out[lines, units:] = (back_hidden * silu_gate).astype(back_out.dtype)
+        return 0
+
+    lax.fori_loop(0, 4, finish, 0)
+
+    @pl.when(sp == 0)
+    def _():
+        head_out[...] = jnp.zeros_like(head_out)
+
+    @pl.when(sp > 0)
+    def _():
+        for which in range(2):
+            copy_to(
+                head_out.at[which],
+                head_out.at[which],
+                small_send.at[3 + which],
+                small_recv.at[4 + which],
+                sp,
+                peer,
+            ).wait_recv()
+
+    @pl.when(sp < 3)
+    def _():
+        head_copy(0).wait_send()
+        head_copy(1).wait_send()
+
+    for at, to_sp in enumerate(others):
+        scale_copy(at, to_sp).wait_send()
     for array in range(2):
-        pltpu.make_async_copy(
-            ins[array], block(array, sp, level, core), own_sem.at[array]
-        ).wait()
         for of_level in range(levels):
-            for kind in (PEER, PEER + 1, PEER + 2, PEER + 3):
-                arrive(array, kind, of_level)
-                left(array, kind, of_level)
-            for kind in (BY_X, BY_Y, HALF_X, HALF_Y):
-                left(array, kind, of_level)
-            pl.when((level < levels - 1) & (level >= of_level))(
-                lambda: left(array, Z_UP, of_level)
-            )
-            pl.when((level > 0) & (level <= of_level))(lambda: left(array, Z_DOWN, of_level))
-
-
-def gather_all(cotangent, mixed_state):
+            store(array, of_level).wait()
+
+
+def gather_all(cotangent, mixed_state, scales, conv_inner, conv_input, gate_w, up_w, down_w):
     rows, cols = cotangent.shape
-    levels = lax.axis_size("tp") // 2
-    whole = jax.ShapeDtypeStruct((4 * rows, 2 * levels * cols), cotangent.dtype)
+    units, width = gate_w.shape
+    narrow = cotangent.dtype
+    dma = pltpu.SemaphoreType.DMA
+    vmem = pl.BlockSpec(memory_space=pltpu.VMEM)
+    hbm = pl.BlockSpec(memory_space=pl.ANY)
+    whole = jax.ShapeDtypeStruct((4 * rows, width), narrow)
     return pl.pallas_call(
-        functools.partial(gather_kernel, levels),
-        out_shape=(whole, whole),
-        in_specs=[pl.BlockSpec(memory_space=pltpu.VMEM)] * 2,
-        out_specs=[pl.BlockSpec(memory_space=pl.ANY)] * 2,
+        gather_kernel,
+        out_shape=(
+            whole,
+            whole,
+            jax.ShapeDtypeStruct((4 * rows, units), narrow),
+            jax.ShapeDtypeStruct((4 * rows, 2 * units), narrow),
+            jax.ShapeDtypeStruct((2, conv_inner.shape[0], 128), narrow),
+        ),
+        in_specs=[vmem] * 5 + [hbm] * 3,
+        out_specs=[hbm, hbm, vmem, vmem, vmem],
         scratch_shapes=[
-            pltpu.SemaphoreType.DMA((2,)),
-            pltpu.SemaphoreType.DMA((2, KINDS, levels)),
-            pltpu.SemaphoreType.DMA((2, KINDS, levels)),
+            pltpu.VMEM((4 * rows, width), narrow),
+            pltpu.VMEM((4 * rows, width), narrow),
+            pltpu.VMEM((units, width), narrow),
+            pltpu.VMEM((units, width), narrow),
+            pltpu.VMEM((units, width), narrow),
+            pltpu.VMEM((4 * rows, units), jnp.float32),
+            pltpu.VMEM((4 * rows, units), jnp.float32),
+            pltpu.VMEM((4 * rows, units), jnp.float32),
+            pltpu.VMEM((4, 8, rows), jnp.float32),
+            dma((2,)),
+            dma((3,)),
+            dma((2, LEVELS)),
+            dma((5,)),
+            dma((6,)),
+            dma((2, KINDS, LEVELS)),
+            dma((2, KINDS, LEVELS)),
         ],
-        compiler_params=pltpu.CompilerParams(collective_id=0, has_side_effects=True),
+        compiler_params=pltpu.CompilerParams(
+            collective_id=0, has_side_effects=True, vmem_limit_bytes=63 * 1024 * 1024
+        ),
         name="gather_all",
-    )(cotangent, mixed_state)
+    )(cotangent, mixed_state, scales, conv_inner, conv_input, gate_w, up_w, down_w)
 
 
 PIECES = 2
@@ -662,23 +862,26 @@
     )(back, gate_w, up_w, cotangent, act)
 
 
-def outer_kernel(hidden_ref, gate_ref, up_ref, state_ref, cot_ref, g_out, u_out, d_out, turned):
+def outer_kernel(hidden_ref, back_ref, state_ref, cot_ref, g_out, u_out, d_out, turned):
+    units = hidden_ref.shape[1]
+
     @pl.when(pl.program_id(0) == 0)
     def _():
         turned[0] = hidden_ref[...].T
-        turned[1] = gate_ref[...].T
-        turned[2] = up_ref[...].T
+        turned[1] = back_ref[:, :units].T
+        turned[2] = back_ref[:, units:].T
 
     d_out[...] = jnp.dot(turned[0], cot_ref[...], preferred_element_type=jnp.float32)
     g_out[...] = jnp.dot(turned[1], state_ref[...], preferred_element_type=jnp.float32)
     u_out[...] = jnp.dot(turned[2], state_ref[...], preferred_element_type=jnp.float32)
 
 
-def weight_grads(hidden, back_gate, back_up, state, cot):
+def weight_grads(hidden, back, state, cot):
     rows, units = hidden.shape
     width = state.shape[1]
     tile = min(512, width)
     whole = pl.BlockSpec((rows, units), lambda i: (0, 0))
+    double = pl.BlockSpec((rows, 2 * units), lambda i: (0, 0))
     tall = pl.BlockSpec((rows, tile), lambda i: (0, i))
     flat = pl.BlockSpec((units, tile), lambda i: (0, i))
     out = jax.ShapeDtypeStruct((units, width), jnp.float32)
@@ -686,7 +889,7 @@
         outer_kernel,
         grid=(width // tile,),
         out_shape=(out, out, out),
-        in_specs=[whole, whole, whole, tall, tall],
+        in_specs=[whole, double, tall, tall],
         out_specs=[flat, flat, flat],
         scratch_shapes=[pltpu.VMEM((3, units, rows), jnp.bfloat16)],
         cost_estimate=pl.CostEstimate(
@@ -695,18 +898,16 @@
             transcendentals=0,
         ),
         name="weight_grads",
-    )(hidden, back_gate, back_up, state, cot)
-
-
-def conv_forward(conv_outer, conv_inner, conv_input, conv_taps):
+    )(hidden, back, state, cot)
+
+
+def conv_head(conv_inner, conv_input, rim_width):
+    return from_behind(jnp.stack([conv_inner[:, -rim_width:], conv_input[:, -rim_width:]]), "sp", 1)
+
+
+def conv_forward(conv_outer, conv_inner, conv_input, conv_taps, head_block):
     tok_count = conv_inner.shape[1]
     taps_count = conv_taps.shape[0]
-    rim_width = taps_count - 1
-    head_block = from_behind(
-        jnp.stack([conv_inner[:, tok_count - rim_width :], conv_input[:, tok_count - rim_width :]]),
-        "sp",
-        1,
-    )
     inner_ext = jnp.concatenate([head_block[0], conv_inner], axis=1).astype(jnp.float32)
     input_ext = jnp.concatenate([head_block[1], conv_input], axis=1).astype(jnp.float32)
     inner_prod = inner_ext * input_ext
@@ -757,31 +958,19 @@
     gate_w, up_w, down_w = w_gate[0], w_up[0], w_down[0]
     choice = route_ids[:, :, None] == jnp.arange(experts, dtype=jnp.int32)[None, None, :]
     scale_of = jnp.sum(jnp.where(choice, route_weights[:, :, None], 0.0), axis=1).T
-    scales = lax.all_to_all(
-        scale_of[:, None], "sp", split_axis=0, concat_axis=1, tiled=True
-    ).reshape(-1, 1)
-    conv_out, outer_f, mixer_act = conv_forward(conv_outer, conv_inner, conv_input, conv_taps)
-    cot_all, rows_in = gather_all(cotangent, mixed_state)
-    gate_pre = jnp.einsum("rd,fd->rf", rows_in, gate_w, preferred_element_type=jnp.float32)
-    up_pre = jnp.einsum("rd,fd->rf", rows_in, up_w, preferred_element_type=jnp.float32)
-    back_hidden = scales * jnp.einsum(
-        "rd,fd->rf", cot_all, down_w, preferred_element_type=jnp.float32
-    )
-    sig_gate = jax.nn.sigmoid(gate_pre)
-    silu_gate = gate_pre * sig_gate
-    hidden = (scales * (silu_gate * up_pre)).astype(jnp.bfloat16)
-    back_gate = (back_hidden * up_pre * sig_gate * (1.0 + gate_pre * (1.0 - sig_gate))).astype(
-        jnp.bfloat16
-    )
-    back_up = (back_hidden * silu_gate).astype(jnp.bfloat16)
-    grad_mixed, tokens, quarter, act_all = reduce_all(
-        jnp.concatenate([back_gate, back_up], axis=1), gate_w, up_w, cotangent, mixer_act
-    )
+    scales = jnp.broadcast_to(scale_of[:, None, :], (experts, 8, scale_of.shape[1]))
+    cot_all, rows_in, hidden, back, head = gather_all(
+        cotangent, mixed_state, scales, conv_inner, conv_input, gate_w, up_w, down_w
+    )
+    rim_width = conv_taps.shape[0] - 1
+    conv_out, outer_f, mixer_act = conv_forward(
+        conv_outer, conv_inner, conv_input, conv_taps, head[:, :, -rim_width:]
+    )
+    grad_mixed, tokens, quarter, act_all = reduce_all(back, gate_w, up_w, cotangent, mixer_act)
     back_mixer = jnp.einsum("cd,td->ct", out_proj, tokens, preferred_element_type=jnp.float32)
     grad_proj = jnp.dot(act_all, quarter, preferred_element_type=jnp.float32)
-    grad_gate_e, grad_up_e, grad_down_e = weight_grads(
-        hidden, back_gate, back_up, rows_in, cot_all
-    )
+    tokens, hidden = lax.optimization_barrier((tokens, hidden))
+    grad_gate_e, grad_up_e, grad_down_e = weight_grads(hidden, back, rows_in, cot_all)
     grad_outer, grad_inner, grad_input = conv_backward(
         back_mixer, conv_out, outer_f, conv_inner, conv_input, conv_taps
     )
@@ -854,7 +1043,13 @@
     ).reshape(experts * capacity, col_count)
     picked = arrived[slot_dest].astype(jnp.float32).reshape(tok_count, top_count, col_count)
     grad_mixed = (cotangent.astype(jnp.float32) + jnp.sum(picked, axis=1)).astype(jnp.bfloat16)
-    conv_out, outer_f, mixer_act = conv_forward(conv_outer, conv_inner, conv_input, conv_taps)
+    conv_out, outer_f, mixer_act = conv_forward(
+        conv_outer,
+        conv_inner,
+        conv_input,
+        conv_taps,
+        conv_head(conv_inner, conv_input, conv_taps.shape[0] - 1),
+    )
     full_back = lax.all_gather(grad_mixed, "tp", axis=1, tiled=True)
     back_mixer = jnp.einsum("cd,td->ct", out_proj, full_back, preferred_element_type=jnp.float32)
     proj_term = jnp.dot(mixer_act, full_back, preferred_element_type=jnp.float32)

time: 210 us -> 174 us (0.83)
  matrix products: 19.4 us -> 3.08 us
  Pallas kernels: 170 us -> 161 us
  starting transfers between devices: 6.35 us -> 1.94 us
  local copies, waits for them, and re-layouts: 5.17 us -> 2.45 us
    dot_general x3 -> x0, matrix products: 17 us -> none  [the longest x1 7.1 us: whole_rows(): jnp.einsum('rd,fd->rf', cot_all, down_w, preferred_element_type=jnp.float32)]
    pallas_call x1, Pallas kernels: 77.1 us -> 69 us  [gather_all(): pl.pallas_call(gather_kernel, out_shape=(whole, whole, jax.ShapeDtypeStru...]
    all_to_all x1 -> x0, starting transfers between devices: 3.63 us -> none  [whole_rows(): lax.all_to_all(scale_of[:, None], 'sp', split_axis=0, concat_axis=1, tile...]
  transfers between devices with their start and end apart: 3 -> 1, of which waited for: 1 -> 0; matrix products, arithmetic and copies ran while one was open for 7% -> 1% of each run, Pallas kernels for 37% -> 9%
where the time goes in v2:
time: 174 us; the launch traced here: 173 us
  Pallas kernels  161 us (93%)
  other arithmetic  3.9 us (2%)
  matrix products  3.08 us (2%)
  local copies, waits for them, and re-layouts  2.45 us (1%)
  starting transfers between devices  1.94 us (1%)
    pallas_call x1, Pallas kernels, reduce_all(): pl.pallas_call(reduce_kernel, out_shape=(jax.ShapeDtypeStruct((rows, half...  76.2 us
    pallas_call x1, Pallas kernels, gather_all(): pl.pallas_call(gather_kernel, out_shape=(whole, whole, jax.ShapeDtypeStru...  69 us
    pallas_call x1, Pallas kernels, weight_grads(): pl.pallas_call(outer_kernel, grid=(width // tile,), out_shape=(out, out,...  16.1 us
  transfers between devices with their start and end apart: 1, of which 0 were waited for; matrix products, arithmetic and copies ran while one was open for 1% of the time, Pallas kernels for 9%

profile of v2, /device:TPU:7, one launch (start us, length us, event | category | flops | bytes accessed | tf_op | source)
XLA Modules:
  0.0 173.4 jit_solution(9616365837372408544)
XLA Ops:
  0.6 0.7 select_reduce_fusion
  1.3 0.6 broadcast_in_dim.32.scale_in
  2.0 0.0 copy-start.7
  2.0 0.0 copy-start.4
  2.0 0.0 copy-start.5
  2.0 0.0 copy-start.6
  2.0 69.0 %gather_all.1 = (bf16[1024,4096]{1,0:T(8,128)(2,1)}, bf16[1024,4096]{1,0:T(8,128)(2,1)}, bf16[1024,256]{1,0:T(8,128)(2,1)}, bf16[1024,512]{1,0:T(8,128)(2,1)}, bf16[2,256,128]{2,1,0:T(8,128)(2,1)}) custom-call(bf16[256,512]{1,0:T(8,128)(2,1)} %cot_in.3, bf16[256,512]{1,0:T(8,128)(2,1)} %state_in.1, f32[4,8,256]{2,1,0:T(8,128)} %broadcast_in_dim.32.scale_in, ...), custom_call_target="tpu_custom_call" | custom-call | tf_op jit(solution)/shard_map/gather_all/pallas_call | solution.py:403
  71.0 0.0 copy-start
  71.0 0.0 copy-start.1
  71.1 1.1 slice_bitcast_fusion
  72.1 0.0 copy-done.7
  72.2 0.0 copy-done.4
  72.2 0.0 copy-done.5
  72.2 0.2 convert_multiply_fusion
  72.4 0.0 copy-done.6
  72.4 0.3 fusion
  72.7 0.0 copy-done
  72.7 0.0 copy-done.1
  72.7 0.0 copy-start.3
  72.7 76.2 %reduce_all.1 = (bf16[256,512]{1,0:T(8,128)(2,1)S(1)}, bf16[256,4096]{1,0:T(8,128)(2,1)S(1)}, bf16[1024,1024]{1,0:T(8,128)(2,1)}, bf16[256,1024]{1,0:T(8,128)(2,1)S(1)}) custom-call(bf16[1024,512]{1,0:T(8,128)(2,1)S(1)} %copy-done.1, bf16[256,4096]{1,0:T(8,128)(2,1)} %bitcast.21, bf16[256,4096]{1,0:T(8,128)(2,1)} %bitcast.23, bf16[256,512]{1,0:T(8,128)(2,1)S(1)} %copy-done, ...), custom_call_target="tpu_custom_call" | custom-call | tf_op jit(solution)/shard_map/reduce_all/pallas_call | solution.py:820
  148.9 0.0 copy-done.3
  148.9 1.4 convert_multiply_fusion.1
  150.3 1.9 %collective-permute-start = (f32[256,2]{1,0:T(8,128)S(1)}, f32[256,2]{1,0:T(8,128)}, u32[]{:S(2)}, u32[]{:S(2)}) collective-permute-start(f32[256,2]{1,0:T(8,128)S(1)} %slice.53), channel_id=1, source_target_pairs={{8,0},{16,8},{24,16},{9,1},{17,9},{25,17},{10,2},{18,10},{26,18},{... | collective-permute-start | bytes 6152 | tf_op jit(solution)/shard_map/ppermute | solution.py:14
  152.2 0.0 copy-start.2
  152.2 16.1 %weight_grads.1 = (f32[256,4096]{1,0:T(8,128)}, f32[256,4096]{1,0:T(8,128)}, f32[256,4096]{1,0:T(8,128)}) custom-call(bf16[1024,256]{1,0:T(8,128)(2,1)} %get-tuple-element.25.hidden_ref, bf16[1024,512]{1,0:T(8,128)(2,1)} %get-tuple-element.21.back_in.back_ref, bf16[1024,4096]{1,0:T(8,128)(2,1)} %get-tuple-element.26.state_ref, ...), custom_call_target="tpu_custom_call" | custom-call | flops 6442450944 | bytes 29360128 | tf_op jit(solution)/shard_map/weight_grads/pallas_call | solution.py:888
  168.4 0.0 copy-done.2
  168.4 1.7 fusion.11
  170.0 0.0 collective-permute-done
  170.0 2.0 %multiply_convert_fusion = (bf16[256,256]{1,0:T(8,128)(2,1)}, f32[256,256]{1,0:T(8,128)S(1)}) fusion(bf16[256,256]{1,0:T(8,128)(2,1)S(1)} %copy-done.4, f32[256,256]{1,0:T(8,128)S(1)} %get-tuple-element.38, f32[256]{0:T(256)S(1)} %bitcast.29, f32[256,2]{1,0:T(8,128)} %collective-permute-done, f32[256]{0:T(256)S(1)} %bitcast.31, f32[256]{0:T(256)S(1)} %bitcast.27), kind=kLoop, calls=%fused_computation.18 | loop fusion | flops 655360 | bytes 791552 | tf_op jit(solution)/shard_map/convert_element_type | solution.py:939
  172.1 0.7 multiply_convert_fusion.1
  172.7 0.7 copy.26
  (2 shorter events, 0.0 us)
Async XLA Ops:
  2.0 70.2 %copy-start.7 = (f32[3,256]{1,0:T(4,128)S(1)}, f32[3,256]{1,0:T(4,128)}, u32[]{:S(2)}) copy-start(f32[3,256]{1,0:T(4,128)} %param.15) | copy-start | bytes 9220
  2.0 70.2 %copy-start.4 = (bf16[256,256]{1,0:T(8,128)(2,1)S(1)}, bf16[256,256]{1,0:T(8,128)(2,1)}, u32[]{:S(2)}) copy-start(bf16[256,256]{1,0:T(8,128)(2,1)} %inner_in.1) | copy-start | bytes 393220
  2.0 70.2 %copy-start.5 = (bf16[256,256]{1,0:T(8,128)(2,1)S(1)}, bf16[256,256]{1,0:T(8,128)(2,1)}, u32[]{:S(2)}) copy-start(bf16[256,256]{1,0:T(8,128)(2,1)} %input_in.1) | copy-start | bytes 393220
  2.0 70.4 %copy-start.6 = (bf16[256,256]{1,0:T(8,128)(2,1)S(1)}, bf16[256,256]{1,0:T(8,128)(2,1)}, u32[]{:S(2)}) copy-start(bf16[256,256]{1,0:T(8,128)(2,1)} %param.12) | copy-start | bytes 393220
  71.0 1.7 copy-start
  71.0 1.7 copy-start.1
  72.7 76.2 %copy-start.3 = (bf16[256,4096]{1,0:T(8,128)(2,1)S(1)}, bf16[256,4096]{1,0:T(8,128)(2,1)}, u32[]{:S(2)}) copy-start(bf16[256,4096]{1,0:T(8,128)(2,1)} %param.16) | copy-start | bytes 6291460
  150.3 19.7 %collective-permute-start = (f32[256,2]{1,0:T(8,128)S(1)}, f32[256,2]{1,0:T(8,128)}, u32[]{:S(2)}, u32[]{:S(2)}) collective-permute-start(f32[256,2]{1,0:T(8,128)S(1)} %slice.53), channel_id=1, source_target_pairs={{8,0},{16,8},{24,16},{9,1},{17,9},{25,17},{10,2},{18,10},{26,18},{... | collective-permute-start | bytes 6152 | tf_op jit(solution)/shard_map/ppermute | solution.py:14
  152.2 16.1 %copy-start.2 = (bf16[1024,1024]{1,0:T(8,128)(2,1)S(1)}, bf16[1024,1024]{1,0:T(8,128)(2,1)}, u32[]{:S(2)}) copy-start(bf16[1024,1024]{1,0:T(8,128)(2,1)} %get-tuple-element.33) | copy-start | bytes 6291460
